TPU v7x, 32 devices: a whole 2x2x4 slice. The times are simulated.
32 devices in a mesh: sp: 8 (over z, y), tp: 4 (over x, core).
Axes of the slice: x: 2, y: 2, z: 4, core: 2. Of those that a mesh axis runs over, the one named last changes fastest.
Arguments:
- activations: bfloat16 [6144, 2048], P(('sp', 'tp')), may hold values from -6 to 6
- in_gain: float32 [2048], replicated, may hold values from 0.1 to 1.9
- w_pool_in: bfloat16 [2048, 1024], P(None, 'tp'), may hold values from -0.125 to 0.125
- pool_gain: float32 [1024], P('tp'), may hold values from 0.1 to 1.9
- w_qlat: bfloat16 [2048, 768], P(None, 'tp'), may hold values from -0.125 to 0.125
- w_kvlat: bfloat16 [2048, 512], P(None, 'tp'), may hold values from -0.125 to 0.125
- w_krope: bfloat16 [2048, 32], replicated, may hold values from -0.125 to 0.125
- qlat_gain: float32 [768], replicated, may hold values from 0.1 to 1.9
- kvlat_gain: float32 [512], replicated, may hold values from 0.1 to 1.9
- w_qup: bfloat16 [768, 1536], P(None, 'tp'), may hold values from -0.21875 to 0.21875
- w_kup: bfloat16 [512, 1024], P(None, 'tp'), may hold values from -0.25 to 0.25
- w_vup: bfloat16 [512, 1024], P(None, 'tp'), may hold values from -0.25 to 0.25
- qhead_gain: float32 [96], replicated, may hold values from 1.1 to 1.9
- khead_gain: float32 [96], replicated, may hold values from 1.1 to 1.9
- w_out_pool: bfloat16 [1024, 2048], P('tp'), may hold values from -0.1875 to 0.1875
- w_out_attn: bfloat16 [1024, 2048], P('tp'), may hold values from -0.75 to 0.75
Outputs:
- mixed: bfloat16 [6144, 2048], P(('sp', 'tp'))
All inputs are finite; a program needn't handle non-finite values.
Results may differ from a plain program's by a relative error of at most 0.025.
Values may be sent and summed in bfloat16 or wider, within the bound.
A program may use at most 128 MiB of HBM per device.

v0:
```python
import functools
import math

import jax
import jax.numpy as jnp
from jax import lax
from jax.experimental import pallas as pl
from jax.experimental.pallas import tpu as pltpu
from jax.sharding import PartitionSpec as P

GROUP = 256
NOPE = 64
ROPE = 32
VDIM = 64
HEAD = NOPE + ROPE
LANES = 128

norm_eps = 1e-06
rope_theta = 10000.0
rim_depth = 15
bf16 = jnp.bfloat16
f32 = jnp.float32


def from_behind(block, axis, distance):
    devices = range(lax.axis_size(axis))
    route = [(i - distance, i) for i in devices if i - distance in devices]
    return lax.ppermute(block, axis, route)


def row_norm(source, norm_gain):
    as_float = source.astype(f32)
    factor = lax.rsqrt(jnp.mean(as_float * as_float, axis=-1, keepdims=True) + norm_eps)
    return as_float * factor * norm_gain


def pool_mix(extended, positions, channel_start):
    row_count = positions.shape[0]
    width = extended.shape[1]
    channel = channel_start + jnp.arange(width, dtype=jnp.int32)
    window = jnp.left_shift(jnp.int32(2), channel // GROUP)
    as_float = extended.astype(f32)
    total = as_float
    window_sum = None
    for level in range(4):
        span = 1 << level
        total = total + jnp.concatenate([jnp.zeros((span, width), f32), total[:-span]], axis=0)
        chosen = total[rim_depth:]
        if window_sum is None:
            window_sum = chosen
        else:
            window_sum = jnp.where(window[None, :] >= 2 * span, chosen, window_sum)
    divisor = jnp.minimum(positions[:, None] + 1, window[None, :]).astype(f32)
    return window_sum / divisor - as_float[rim_depth:]


def pad_heads(weight_ref, padded_ref, width):
    weight = weight_ref[...].astype(f32)
    padded_ref[...] = jnp.zeros_like(padded_ref)
    for h in range(weight.shape[1] // width):
        head = weight[:, h * width : (h + 1) * width]
        padded_ref[:, h * LANES : h * LANES + width] = head.astype(bf16)


def pad_row(gain):
    return jnp.pad(gain, (0, LANES - gain.shape[0])).reshape(1, LANES)


def rope_tables(rows, blocks):
    half = ROPE // 2
    frequency = rope_theta ** (-jnp.arange(0, ROPE, 2, dtype=f32) / ROPE)

    def make(positions):
        angles = positions.astype(f32)[:, None] * frequency[None, :]
        cosine, sine = jnp.cos(angles), jnp.sin(angles)
        count = positions.shape[0]
        rest = LANES - HEAD
        cos_row = jnp.concatenate(
            [jnp.ones((count, NOPE), f32), cosine, cosine, jnp.zeros((count, rest), f32)], axis=1
        )
        sin_row = jnp.concatenate(
            [jnp.zeros((count, NOPE), f32), sine, sine, jnp.zeros((count, rest), f32)], axis=1
        )
        return cos_row, sin_row

    return make(jnp.arange(rows)) + make(jnp.arange(blocks) * rows)


def head_finish(x, gain, cosine, sin_low, sin_high):
    factor = lax.rsqrt(jnp.sum(x * x, axis=1, keepdims=True) * (1.0 / HEAD) + norm_eps)
    y = x * factor * gain
    half = ROPE // 2
    return (
        y * cosine
        + pltpu.roll(y, LANES - half, 1) * sin_low
        + pltpu.roll(y, half, 1) * sin_high
    )


def attention_kernel(
    heads,
    step_rows,
    q_ref,
    kv_ref,
    own_ref,
    wq_raw,
    wk_raw,
    wv_raw,
    qlat_gain,
    kvlat_gain,
    qh_gain,
    kh_gain,
    cos_r,
    sin_r,
    cos_b,
    sin_b,
    out_ref,
    kv_buf,
    queries,
    keys_t,
    values,
    acc,
    own_buf,
    wq_ref,
    wk_ref,
    wv_ref,
    sem,
    own_sem,
):
    rows = q_ref.shape[0]
    kvlat = wk_ref.shape[0]
    mine = lax.axis_index("sp")
    lane = lax.broadcasted_iota(jnp.int32, (step_rows, LANES), 1)
    score_scale = HEAD ** (-0.5) * math.log2(math.e)

    def fetch(block, slot):
        return pltpu.make_async_copy(kv_ref.at[block], kv_buf.at[slot], sem.at[slot])

    own_copy = pltpu.make_async_copy(own_ref, own_buf, own_sem)
    own_copy.start()

    @pl.when(mine > 0)
    def _():
        fetch(0, 0).start()

    pad_heads(wq_raw, wq_ref, HEAD)
    pad_heads(wk_raw, wk_ref, NOPE)
    pad_heads(wv_raw, wv_ref, VDIM)

    def angles(block, at):
        cr, sr = cos_r[at, :], sin_r[at, :]
        cb, sb = cos_b[pl.ds(block, 1), :], sin_b[pl.ds(block, 1), :]
        cosine = jnp.where(lane < NOPE, 1.0, cr * cb - sr * sb)
        sine = sr * cb + cr * sb
        low = jnp.where((lane >= NOPE) & (lane < NOPE + ROPE // 2), -sine, 0.0)
        high = jnp.where((lane >= NOPE + ROPE // 2) & (lane < HEAD), sine, 0.0)
        return cosine, low, high

    def prepare_queries(step, _):
        at = pl.ds(pl.multiple_of(step * step_rows, step_rows), step_rows)
        normed = row_norm(q_ref[at, :], qlat_gain[...]).astype(bf16)
        raw = jnp.dot(normed, wq_ref[...], preferred_element_type=f32).astype(bf16).astype(f32)
        tables = angles(mine, at)
        for h in range(heads):
            x = raw[:, h * LANES : (h + 1) * LANES]
            y = head_finish(x, qh_gain[...], *tables)
            queries[h, at, :] = (y * score_scale).astype(bf16)
        return 0

    lax.fori_loop(0, rows // step_rows, prepare_queries, 0)
    acc[...] = jnp.zeros_like(acc)

    def prepare_keys(block, source):
        def one(step, _):
            at = pl.ds(pl.multiple_of(step * step_rows, step_rows), step_rows)
            latent = source[at, :kvlat]
            shared = source[at, kvlat:].astype(f32)
            normed = row_norm(latent, kvlat_gain[...]).astype(bf16)
            plain = jnp.dot(normed, wk_ref[...], preferred_element_type=f32).astype(bf16).astype(f32)
            value = jnp.dot(normed, wv_ref[...], preferred_element_type=f32)
            tables = angles(block, at)
            for h in range(heads):
                x = plain[:, h * LANES : (h + 1) * LANES] + shared
                y = head_finish(x, kh_gain[...], *tables)
                keys_t[h, :, at] = y.T.astype(bf16)
                v = jnp.where(lane == VDIM, 1.0, value[:, h * LANES : (h + 1) * LANES])
                values[h, at, :] = v.astype(bf16)
            return 0

        lax.fori_loop(0, rows // step_rows, one, 0)

    def accumulate(on_diagonal):
        def one(step, _):
            at = pl.ds(pl.multiple_of(step * step_rows, step_rows), step_rows)
            for h in range(heads):
                scores = jnp.dot(queries[h, at, :], keys_t[h], preferred_element_type=f32)
                weights = jnp.exp2(scores)
                if on_diagonal:
                    q_pos = step * step_rows + lax.broadcasted_iota(jnp.int32, scores.shape, 0)
                    k_pos = lax.broadcasted_iota(jnp.int32, scores.shape, 1)
                    weights = jnp.where(k_pos <= q_pos, weights, 0.0)
                acc[h, at, :] += jnp.dot(weights.astype(bf16), values[h], preferred_element_type=f32)
            return 0

        lax.fori_loop(0, rows // step_rows, one, 0)

    def earlier(block, _):
        slot = lax.rem(block, 2)
        fetch(block, slot).wait()

        @pl.when(block + 1 < mine)
        def _():
            fetch(block + 1, 1 - slot).start()

        prepare_keys(block, kv_buf.at[slot])
        accumulate(False)
        return 0

    lax.fori_loop(0, mine, earlier, 0)
    own_copy.wait()
    prepare_keys(mine, own_buf)
    accumulate(True)

    def finish(step, _):
        at = pl.ds(pl.multiple_of(step * step_rows, step_rows), step_rows)
        parts = []
        for h in range(heads):
            a = acc[h, at, :]
            parts.append(a[:, :VDIM] / a[:, VDIM : VDIM + 1])
        out_ref[at, :] = jnp.concatenate(parts, axis=1).astype(bf16)
        return 0

    lax.fori_loop(0, rows // step_rows, finish, 0)


def attention(q_lat, kv_all, kv_own, wq, wk, wv, gains, tables):
    rows = q_lat.shape[0]
    heads = wq.shape[1] // HEAD
    step_rows = math.gcd(rows, 256)
    vm = pl.BlockSpec(memory_space=pltpu.VMEM)
    return pl.pallas_call(
        functools.partial(attention_kernel, heads, step_rows),
        out_shape=jax.ShapeDtypeStruct((rows, heads * VDIM), bf16),
        in_specs=[vm, pl.BlockSpec(memory_space=pl.ANY), pl.BlockSpec(memory_space=pl.ANY)] + [vm] * 11,
        out_specs=vm,
        scratch_shapes=[
            pltpu.VMEM((2,) + kv_all.shape[1:], bf16),
            pltpu.VMEM((heads, rows, LANES), bf16),
            pltpu.VMEM((heads, LANES, rows), bf16),
            pltpu.VMEM((heads, rows, LANES), bf16),
            pltpu.VMEM((heads, rows, LANES), f32),
            pltpu.VMEM(kv_own.shape, bf16),
            pltpu.VMEM((wq.shape[0], heads * LANES), bf16),
            pltpu.VMEM((wk.shape[0], heads * LANES), bf16),
            pltpu.VMEM((wv.shape[0], heads * LANES), bf16),
            pltpu.SemaphoreType.DMA((2,)),
            pltpu.SemaphoreType.DMA,
        ],
        compiler_params=pltpu.CompilerParams(vmem_limit_bytes=48 * 1024 * 1024),
    )(q_lat, kv_all, kv_own, wq, wk, wv, *gains, *tables)


MESH = pl.DeviceIdType.MESH


def remote(src, dst, send_sem, recv_sem, target):
    return pltpu.make_async_remote_copy(
        src_ref=src,
        dst_ref=dst,
        send_sem=send_sem,
        recv_sem=recv_sem,
        device_id=target,
        device_id_type=MESH,
    )


def tp_place():
    me = lax.axis_index("tp")
    return me, lax.rem(me, 2), lax.div(me, 2)


def greet_tp(n_tp, me, barrier):
    for step in range(1, n_tp):
        pl.semaphore_signal(
            barrier, inc=1, device_id={"tp": lax.rem(me + step, n_tp)}, device_id_type=MESH
        )


def tp_gather_kernel(n_tp, x_ref, out_ref, local_sem, own_send, far_send, relay_send, recv):
    me, core, chip = tp_place()
    chips = n_tp // 2
    partner = me + 1 - 2 * core
    barrier = pltpu.get_barrier_semaphore()
    greet_tp(n_tp, me, barrier)
    pl.semaphore_wait(barrier, n_tp - 1)
    far = []
    for step in range(1, chips):
        there = 2 * lax.rem(chip + step, chips) + core
        copy = remote(x_ref, out_ref.at[me], far_send.at[step - 1], recv.at[me], {"tp": there})
        copy.start()
        far.append(copy)
    near = remote(x_ref, out_ref.at[me], own_send, recv.at[me], {"tp": partner})
    near.start()
    keep = pltpu.make_async_copy(x_ref, out_ref.at[me], local_sem)
    keep.start()
    relays = []
    for step in range(1, chips):
        source = 2 * lax.rem(chip + chips - step, chips) + core
        remote(x_ref, out_ref.at[source], far_send.at[step - 1], recv.at[source], {"tp": partner}).wait_recv()
        copy = remote(
            out_ref.at[source],
            out_ref.at[source],
            relay_send.at[step - 1],
            recv.at[source],
            {"tp": partner},
        )
        copy.start()
        relays.append(copy)
    for step in range(chips):
        source = 2 * lax.rem(chip + step, chips) + 1 - core
        remote(x_ref, out_ref.at[source], own_send, recv.at[source], {"tp": partner}).wait_recv()
    for copy in far + relays:
        copy.wait_send()
    near.wait_send()
    keep.wait()


def tp_gather(block, identity):
    n_tp = lax.axis_size("tp")
    vm = pl.BlockSpec(memory_space=pltpu.VMEM)
    others = max(1, n_tp // 2 - 1)
    return pl.pallas_call(
        functools.partial(tp_gather_kernel, n_tp),
        out_shape=jax.ShapeDtypeStruct((n_tp,) + block.shape, block.dtype),
        in_specs=[vm],
        out_specs=vm,
        scratch_shapes=[
            pltpu.SemaphoreType.DMA,
            pltpu.SemaphoreType.DMA,
            pltpu.SemaphoreType.DMA((others,)),
            pltpu.SemaphoreType.DMA((others,)),
            pltpu.SemaphoreType.DMA((n_tp,)),
        ],
        compiler_params=pltpu.CompilerParams(collective_id=identity, has_side_effects=True),
    )(block)


def tp_scatter_kernel(
    n_tp, x_ref, out_ref, pair_buf, sum_buf, far_buf, pair_send, pair_recv, far_send, far_recv
):
    me, core, chip = tp_place()
    chips = n_tp // 2
    partner = me + 1 - 2 * core
    rows = out_ref.shape[0]

    def rows_of(place):
        return x_ref.at[pl.ds(pl.multiple_of(place * rows, rows), rows), :]

    barrier = pltpu.get_barrier_semaphore()
    greet_tp(n_tp, me, barrier)
    pl.semaphore_wait(barrier, n_tp - 1)
    pairs = []
    for step in range(1, chips + 1):
        target_chip = lax.rem(chip + step, chips)
        copy = remote(
            rows_of(2 * target_chip + 1 - core),
            pair_buf.at[step - 1],
            pair_send.at[step - 1],
            pair_recv.at[step - 1],
            {"tp": partner},
        )
        copy.start()
        pairs.append(copy)
    far = []
    for step in range(1, chips):
        there = 2 * lax.rem(chip + step, chips) + core
        pairs[step - 1].wait_recv()
        mine = rows_of(there)[...].astype(f32)
        sum_buf[step - 1] = (mine + pair_buf[step - 1].astype(f32)).astype(bf16)
        copy = remote(
            sum_buf.at[step - 1],
            far_buf.at[step - 1],
            far_send.at[step - 1],
            far_recv.at[step - 1],
            {"tp": there},
        )
        copy.start()
        far.append(copy)
    pairs[chips - 1].wait_recv()
    total = rows_of(me)[...].astype(f32) + pair_buf[chips - 1].astype(f32)
    for step in range(1, chips):
        far[step - 1].wait_recv()
        total = total + far_buf[step - 1].astype(f32)
    out_ref[...] = total.astype(bf16)
    for copy in pairs + far:
        copy.wait_send()


def tp_scatter(partial, identity):
    n_tp = lax.axis_size("tp")
    vm = pl.BlockSpec(memory_space=pltpu.VMEM)
    chips = n_tp // 2
    others = max(1, chips - 1)
    rows, width = partial.shape[0] // n_tp, partial.shape[1]
    return pl.pallas_call(
        functools.partial(tp_scatter_kernel, n_tp),
        out_shape=jax.ShapeDtypeStruct((rows, width), bf16),
        in_specs=[vm],
        out_specs=vm,
        scratch_shapes=[
            pltpu.VMEM((chips, rows, width), bf16),
            pltpu.VMEM((others, rows, width), bf16),
            pltpu.VMEM((others, rows, width), bf16),
            pltpu.SemaphoreType.DMA((chips,)),
            pltpu.SemaphoreType.DMA((chips,)),
            pltpu.SemaphoreType.DMA((others,)),
            pltpu.SemaphoreType.DMA((others,)),
        ],
        compiler_params=pltpu.CompilerParams(
            collective_id=identity, has_side_effects=True, vmem_limit_bytes=40 * 1024 * 1024
        ),
    )(partial)


def sp_gather_kernel(
    n_sp, n_tp, x_ref, out_ref, deep_send, side_send, near_send, far_send, relay_send, recv
):
    me, core, chip = tp_place()
    chips = n_tp // 2
    partner = me + 1 - 2 * core
    shard = lax.axis_index("sp")
    deep, side = lax.div(shard, 2), lax.rem(shard, 2)
    last_deep = n_sp // 2 - 1
    rows = x_ref.shape[0] // n_tp
    other = shard + 1 - 2 * side

    def piece(block, place):
        return out_ref.at[block, pl.ds(pl.multiple_of(place * rows, rows), rows), :]

    own = x_ref.at[pl.ds(pl.multiple_of(me * rows, rows), rows), :]

    barrier = pltpu.get_barrier_semaphore()
    greet_tp(n_tp, me, barrier)
    pl.semaphore_signal(barrier, inc=1, device_id={"sp": other}, device_id_type=MESH)

    @pl.when(deep > 0)
    def _():
        pl.semaphore_signal(barrier, inc=1, device_id={"sp": shard - 2}, device_id_type=MESH)

    @pl.when(deep < last_deep)
    def _():
        pl.semaphore_signal(barrier, inc=1, device_id={"sp": shard + 2}, device_id_type=MESH)

    neighbours = jnp.minimum(deep, 1) + jnp.minimum(last_deep - deep, 1)
    pl.semaphore_wait(barrier, n_tp + neighbours)

    def onward(block, source):
        return remote(source, piece(block, me), deep_send.at[block], recv.at[block, me], {"sp": shard + 2})

    def across(block, source):
        return remote(source, piece(block, me), side_send.at[block], recv.at[block, me], {"sp": other})

    def near(block):
        return remote(piece(block, me), piece(block, me), near_send.at[block], recv.at[block, me], {"tp": partner})

    def far(block, step):
        there = 2 * lax.rem(chip + step, chips) + core
        return remote(
            piece(block, me), piece(block, me), far_send.at[block, step - 1], recv.at[block, me], {"tp": there}
        )

    def relay(block, step):
        source = 2 * lax.rem(chip + chips - step, chips) + core
        return remote(
            piece(block, source),
            piece(block, source),
            relay_send.at[block, step - 1],
            recv.at[block, source],
            {"tp": partner},
        )

    def arrived(block, place):
        remote(
            piece(block, place), piece(block, place), near_send.at[block], recv.at[block, place], {"tp": partner}
        ).wait_recv()

    def spread(block):
        for step in range(1, chips):
            far(block, step).start()
        near(block).start()

    def pass_on(block):
        for step in range(1, chips):
            arrived(block, 2 * lax.rem(chip + chips - step, chips) + core)
            relay(block, step).start()

    @pl.when(deep < last_deep)
    def _():
        onward(shard, own).start()

    @pl.when(side == 0)
    def _():
        across(shard, own).start()

    def receive(k, _):
        block = shard - 2 * k
        arrived(block, me)

        @pl.when(deep < last_deep)
        def _():
            onward(block, piece(block, me)).start()

        across(block, piece(block, me)).start()
        spread(block)
        return 0

    def receive_other(k, _):
        block = other - 2 * k
        arrived(block, me)
        spread(block)
        return 0

    first_other = 1 - side

    def step(k, _):
        @pl.when((k > 0) & (k <= deep))
        def _():
            receive(k, 0)

        @pl.when((k >= first_other) & (k <= deep))
        def _():
            receive_other(k, 0)

        before = k - 1

        @pl.when((before > 0) & (before <= deep))
        def _():
            pass_on(shard - 2 * before)

        @pl.when((before >= first_other) & (before <= deep))
        def _():
            pass_on(other - 2 * before)

        return 0

    lax.fori_loop(0, deep + 2, step, 0)

    def drain(block, _):
        for c in range(chips):
            arrived(block, 2 * c + 1 - core)
        for s in range(1, chips):
            far(block, s).wait_send()
            relay(block, s).wait_send()
        near(block).wait_send()
        return 0

    lax.fori_loop(0, shard, drain, 0)

    def drain_sends(k, _):
        block = shard - 2 * k
        source = piece(block, me)

        @pl.when(deep < last_deep)
        def _():
            onward(block, source).wait_send()

        @pl.when((k > 0) | (side == 0))
        def _():
            across(block, source).wait_send()

        return 0

    lax.fori_loop(0, deep + 1, drain_sends, 0)


def sp_gather(block, identity):
    n_sp, n_tp = lax.axis_size("sp"), lax.axis_size("tp")
    others = max(1, n_tp // 2 - 1)
    hbm = pl.BlockSpec(memory_space=pl.ANY)
    return pl.pallas_call(
        functools.partial(sp_gather_kernel, n_sp, n_tp),
        out_shape=jax.ShapeDtypeStruct((n_sp,) + block.shape, block.dtype),
        in_specs=[hbm],
        out_specs=hbm,
        scratch_shapes=[
            pltpu.SemaphoreType.DMA((n_sp,)),
            pltpu.SemaphoreType.DMA((n_sp,)),
            pltpu.SemaphoreType.DMA((n_sp,)),
            pltpu.SemaphoreType.DMA((n_sp, others)),
            pltpu.SemaphoreType.DMA((n_sp, others)),
            pltpu.SemaphoreType.DMA((n_sp, n_tp)),
        ],
        compiler_params=pltpu.CompilerParams(collective_id=identity, has_side_effects=True),
    )(block)


def local(
    activations,
    in_gain,
    w_pool_in,
    pool_gain,
    w_qlat,
    w_kvlat,
    w_krope,
    qlat_gain,
    kvlat_gain,
    w_qup,
    w_kup,
    w_vup,
    qhead_gain,
    khead_gain,
    w_out_pool,
    w_out_attn,
):
    own_input = tp_gather(activations, 0)
    own_input = own_input.reshape(-1, own_input.shape[-1])
    row_count = own_input.shape[0]
    n_sp = lax.axis_size("sp")
    positions = lax.axis_index("sp") * row_count + jnp.arange(row_count, dtype=jnp.int32)
    normed = row_norm(own_input, in_gain).astype(bf16)
    q_part = jnp.dot(normed, w_qlat, preferred_element_type=f32).astype(bf16)
    kv_part = jnp.dot(normed, w_kvlat, preferred_element_type=f32).astype(bf16)
    krope_pad = jnp.pad(w_krope, ((0, 0), (NOPE, LANES - HEAD)))
    rope_key = jnp.dot(normed, krope_pad, preferred_element_type=f32).astype(bf16)
    q_width = q_part.shape[1]
    latents = tp_gather(jnp.concatenate([q_part, kv_part], axis=1), 1)
    q_lat = jnp.concatenate([latents[i, :, :q_width] for i in range(latents.shape[0])], axis=1)
    kv_lat = jnp.concatenate(
        [latents[i, :, q_width:] for i in range(latents.shape[0])] + [rope_key], axis=1
    )
    kv_all = sp_gather(kv_lat, 2)
    pool_in = jnp.dot(normed, w_pool_in, preferred_element_type=f32).astype(bf16)
    prev_rows = from_behind(pool_in[row_count - rim_depth :], "sp", 1)
    extended = jnp.concatenate([prev_rows, pool_in], axis=0)
    channel_start = lax.axis_index("tp") * pool_in.shape[1]
    pool_out = (pool_mix(extended, positions, channel_start) * pool_gain).astype(bf16)
    attended = attention(
        q_lat,
        kv_all,
        kv_lat,
        w_qup,
        w_kup,
        w_vup,
        (qlat_gain.reshape(1, -1), kvlat_gain.reshape(1, -1), pad_row(qhead_gain), pad_row(khead_gain)),
        rope_tables(row_count, n_sp),
    )
    term = jnp.dot(pool_out, w_out_pool, preferred_element_type=f32)
    attn_term = jnp.dot(attended, w_out_attn, preferred_element_type=f32)
    return tp_scatter((term + attn_term).astype(bf16), 3)


def solution(mesh):
    placed = (
        P(("sp", "tp"), None),
        P(),
        P(None, "tp"),
        P("tp"),
        P(None, "tp"),
        P(None, "tp"),
        P(),
        P(),
        P(),
        P(None, "tp"),
        P(None, "tp"),
        P(None, "tp"),
        P(),
        P(),
        P("tp", None),
        P("tp", None),
    )
    return jax.shard_map(
        local, mesh=mesh, in_specs=placed, out_specs=P(("sp", "tp"), None), check_vma=False
    )
```

profile of v0, /device:TPU:28, one launch (start us, length us, event | category | flops | bytes accessed | tf_op | source)
XLA Modules:
  0.0 213.0 jit_solution(9693354098325833766)
XLA Ops:
  0.0 24.7 %shard_map.154 = bf16[4,192,2048]{2,1,0:T(8,128)(2,1)} custom-call(bf16[192,2048]{1,0:T(8,128)(2,1)} %x_ref.1), custom_call_target="tpu_custom_call" | custom-call | tf_op jit(solution)/shard_map/pallas_call | solution.py:332
  24.7 2.6 %multiply_reduce_fusion = f32[4,192]{1,0:T(4,128)S(1)} fusion(bf16[4,192,2048]{2,1,0:T(8,128)(2,1)} %shard_map.154), kind=kLoop, calls=%fused_computation.4 | loop fusion | flops 4717824 | bytes 3148800 | tf_op jit(solution)/shard_map/reduce_sum | solution.py:33
  27.4 2.8 %fusion.1 = bf16[768,2048]{1,0:T(8,128)(2,1)S(1)} fusion(f32[2048]{0:T(1024)S(1)} %copy-done.17, f32[768]{0:T(1024)S(1)} %rsqrt.12, bf16[4,192,2048]{2,1,0:T(8,128)(2,1)} %shard_map.154), kind=kLoop, calls=%fused_computation.2 | loop fusion | flops 6291456 | bytes 6302720 | tf_op jit(solution)/shard_map/convert_element_type | solution.py:620
  30.2 1.0 convolution_convert_fusion
  31.2 0.7 copy-done.10
  31.9 1.4 collective-permute-start
  33.4 1.2 convolution_convert_fusion.1
  34.6 0.2 copy.21
  34.8 2.9 %convolution_convert_fusion.3 = bf16[768,128]{1,0:T(8,128)(2,1)S(1)} fusion(bf16[768,2048]{1,0:T(8,128)(2,1)} %copy-done.9, bf16[2048,128]{1,0:T(8,128)(2,1)S(1)} %copy-done.23), kind=kOutput, calls=%fused_computation.10 | convolution fusion | flops 402751488 | bytes 3866624 | tf_op jit(solution)/shard_map/dot_general | solution.py:622
  37.7 1.0 pad_maximum_fusion.1.x_ref
  38.7 19.8 %shard_map.155 = bf16[4,768,320]{2,1,0:T(8,128)(2,1)} custom-call(bf16[768,320]{1,0:T(8,128)(2,1)} %pad_maximum_fusion.1.x_ref), custom_call_target="tpu_custom_call" | custom-call | tf_op jit(solution)/shard_map/pallas_call | solution.py:332
  58.6 2.6 %slice_bitcast_fusion.3 = (bf16[768,192]{1,0:T(8,128)(2,1)}, bf16[768,192]{1,0:T(8,128)(2,1)}, bf16[768,192]{1,0:T(8,128)(2,1)}, bf16[768,192]{1,0:T(8,128)(2,1)}) fusion(bf16[4,768,320]{2,1,0:T(8,128)(2,1)} %shard_map.155), kind=kLoop, calls=%fused_computation.33 | loop fusion | bytes 2359296 | tf_op jit(solution)/shard_map/squeeze | solution.py:627
  61.1 1.1 bitcast_dynamic-update-slice_fusion.3
  62.3 1.1 bitcast_dynamic-update-slice_fusion.2
  63.5 1.1 bitcast_dynamic-update-slice_fusion.1
  64.6 1.1 bitcast_dynamic-update-slice_fusion
  65.9 1.4 multiply_sine_fusion
  67.5 3.0 %fusion.2.x_ref.own_ref = bf16[768,640]{1,0:T(8,128)(2,1)S(1)} fusion(bf16[768,640]{1,0:T(8,128)(2,1)S(1)} %bitcast_dynamic-update-slice_fusion, bf16[768,2048]{1,0:T(8,128)(2,1)} %copy-done.9, bf16[2048,32]{0,1:T(8,128)(2,1)S(1)} %copy-done.24), kind=kOutput, calls=%fused_computation.9 | convolution fusion | flops 402751488 | bytes 3473408 | tf_op jit(solution)/shard_map/dot_general | solution.py:624
  70.6 1.3 maximum_maximum_fusion.1
  72.1 0.5 pad_maximum_fusion.q_ref
  72.7 51.1 %shard_map.156.kv_ref = bf16[8,768,640]{2,1,0:T(8,128)(2,1)} custom-call(bf16[768,640]{1,0:T(8,128)(2,1)} %copy-done.1), custom_call_target="tpu_custom_call" | custom-call | tf_op jit(solution)/shard_map/pallas_call | solution.py:580
  123.8 1.2 copy-done.2
  125.0 1.0 copy-done.3
  126.0 1.0 copy-done.4
  127.0 1.1 copy-done.5
  128.1 0.9 copy-done.7
  129.0 57.3 %shard_map.157 = bf16[768,256]{1,0:T(8,128)(2,1)S(1)} custom-call(bf16[768,768]{1,0:T(8,128)(2,1)S(1)} %pad_maximum_fusion.q_ref, bf16[8,768,640]{2,1,0:T(8,128)(2,1)} %shard_map.156.kv_ref, bf16[768,640]{1,0:T(8,128)(2,1)S(1)} %copy-done.2, bf16[768,384]{1,0:T(8,128)(2,1)S(1)} %copy-done.5, bf16[512,256]{1,0:T(8,128)(2,1)S(1)} %copy-done.6, ...), custom_call_target="tpu_custom_call" | custom-call | tf_op jit(solution)/shard_map/pallas_call | solution.py:241
  186.9 0.4 copy-done.25
  187.3 1.4 fusion.9
  188.7 1.0 add_convert_fusion.x_ref
  189.7 22.4 %shard_map.158 = bf16[192,2048]{1,0:T(8,128)(2,1)S(1)} custom-call(bf16[768,2048]{1,0:T(8,128)(2,1)S(1)} %add_convert_fusion.x_ref), custom_call_target="tpu_custom_call" | custom-call | tf_op jit(solution)/shard_map/pallas_call | solution.py:405
  212.1 0.9 copy.31
  (71 shorter events, 1.1 us)
Async XLA Ops:
  0.0 186.9 %copy-start = (bf16[256,2048]{1,0:T(8,128)(2,1)S(1)}, bf16[256,2048]{1,0:T(8,128)(2,1)}, u32[]{:S(2)}) copy-start(bf16[256,2048]{1,0:T(8,128)(2,1)} %param.30) | copy-start | bytes 3145732
  0.0 27.4 %copy-start.17 = (f32[2048]{0:T(1024)S(1)}, f32[2048]{0:T(1024)}, u32[]{:S(2)}) copy-start(f32[2048]{0:T(1024)} %param.17) | copy-start | bytes 24580
  27.4 2.8 %copy-start.21 = (bf16[2048,256]{1,0:T(8,128)(2,1)S(1)}, bf16[2048,256]{1,0:T(8,128)(2,1)}, u32[]{:S(2)}) copy-start(bf16[2048,256]{1,0:T(8,128)(2,1)} %param.18) | copy-start | bytes 3145732
  30.2 3.2 %copy-start.9 = (bf16[768,2048]{1,0:T(8,128)(2,1)}, bf16[768,2048]{1,0:T(8,128)(2,1)S(1)}, u32[]{:S(2)}) copy-start(bf16[768,2048]{1,0:T(8,128)(2,1)S(1)} %fusion.1) | copy-start | bytes 9437188
  30.2 3.2 %copy-start.22 = (bf16[2048,192]{0,1:T(8,128)(2,1)S(1)}, bf16[2048,192]{0,1:T(8,128)(2,1)}, u32[]{:S(2)}) copy-start(bf16[2048,192]{0,1:T(8,128)(2,1)} %param.20) | copy-start | bytes 2359300
  31.2 0.8 copy-start.10
  31.9 2.9 %copy-start.23 = (bf16[2048,128]{1,0:T(8,128)(2,1)S(1)}, bf16[2048,128]{1,0:T(8,128)(2,1)}, u32[]{:S(2)}) copy-start(bf16[2048,128]{1,0:T(8,128)(2,1)} %param.21) | copy-start | bytes 1572868
  31.9 154.4 %collective-permute-start = (bf16[15,256]{1,0:T(8,128)(2,1)S(1)}, bf16[15,256]{1,0:T(8,128)(2,1)S(1)}, u32[]{:S(2)}, u32[]{:S(2)}) collective-permute-start(bf16[15,256]{1,0:T(8,128)(2,1)S(1)} %slice.72), channel_id=1, source_target_pairs={{0,4},{4,8},{8,12},{12,16},{16,20},{20,24},{24,28},{1,5},{5,9},{9,... | collective-permute-start | bytes 23048 | tf_op jit(solution)/shard_map/ppermute | solution.py:28
  58.5 8.9 %copy-start.24 = (bf16[2048,32]{0,1:T(8,128)(2,1)S(1)}, bf16[2048,32]{0,1:T(8,128)(2,1)}, u32[]{:S(2)}) copy-start(bf16[2048,32]{0,1:T(8,128)(2,1)} %param.22) | copy-start | bytes 393220
  67.5 4.5 %copy-start.19 = (f32[96]{0:T(128)S(1)}, f32[96]{0:T(128)}, u32[]{:S(2)}) copy-start(f32[96]{0:T(128)} %param.29) | copy-start | bytes 1156
  67.5 4.5 %copy-start.20 = (f32[96]{0:T(128)S(1)}, f32[96]{0:T(128)}, u32[]{:S(2)}) copy-start(f32[96]{0:T(128)} %param.28) | copy-start | bytes 1156
  67.5 4.5 %copy-start.12 = (bf16[768,192]{1,0:T(8,128)(2,1)S(1)}, bf16[768,192]{1,0:T(8,128)(2,1)}, u32[]{:S(2)}) copy-start(bf16[768,192]{1,0:T(8,128)(2,1)} %get-tuple-element.5) | copy-start | bytes 884740
  67.5 4.5 %copy-start.13 = (bf16[768,192]{1,0:T(8,128)(2,1)S(1)}, bf16[768,192]{1,0:T(8,128)(2,1)}, u32[]{:S(2)}) copy-start(bf16[768,192]{1,0:T(8,128)(2,1)} %get-tuple-element.6) | copy-start | bytes 884740
  67.5 4.5 %copy-start.14 = (bf16[768,192]{1,0:T(8,128)(2,1)S(1)}, bf16[768,192]{1,0:T(8,128)(2,1)}, u32[]{:S(2)}) copy-start(bf16[768,192]{1,0:T(8,128)(2,1)} %get-tuple-element.7) | copy-start | bytes 884740
  67.5 4.5 %copy-start.15 = (bf16[768,192]{1,0:T(8,128)(2,1)S(1)}, bf16[768,192]{1,0:T(8,128)(2,1)}, u32[]{:S(2)}) copy-start(bf16[768,192]{1,0:T(8,128)(2,1)} %get-tuple-element.8) | copy-start | bytes 884740
  70.6 2.0 copy-start.1
  72.6 51.2 %copy-start.18 = (f32[768]{0:T(1024)S(1)}, f32[768]{0:T(1024)}, u32[]{:S(2)}) copy-start(f32[768]{0:T(1024)} %param.23) | copy-start | bytes 9220
  72.6 51.2 %copy-start.6 = (bf16[512,256]{1,0:T(8,128)(2,1)S(1)}, bf16[512,256]{1,0:T(8,128)(2,1)}, u32[]{:S(2)}) copy-start(bf16[512,256]{1,0:T(8,128)(2,1)} %wk_raw.1) | copy-start | bytes 786436
  72.6 51.2 %copy-start.8 = (f32[512]{0:T(512)S(1)}, f32[512]{0:T(512)}, u32[]{:S(2)}) copy-start(f32[512]{0:T(512)} %param.24) | copy-start | bytes 6148
  123.8 1.2 copy-start.2
  125.0 1.0 copy-start.3
  126.0 1.0 copy-start.4
  127.0 1.1 copy-start.5
  128.1 0.9 copy-start.7
  129.0 57.3 %copy-start.11 = (bf16[768,256]{1,0:T(8,128)(2,1)S(1)}, bf16[768,256]{1,0:T(8,128)(2,1)}, u32[]{:S(2)}) copy-start(bf16[768,256]{1,0:T(8,128)(2,1)} %copy-done.10) | copy-start | bytes 1179652
  186.6 0.7 copy-start.25
  187.3 1.4 copy-start.16
where the time goes:
time: 214 us; the launch traced here: 213 us
  Pallas kernels  175 us (82%)
  local copies, waits for them, and re-layouts  14.8 us (7%)
  matrix products  10.5 us (5%)
  other arithmetic  10.4 us (5%)
    pallas_call x1, Pallas kernels, attention(): pl.pallas_call(functools.partial(attention_kernel, heads, step_rows), out...  57.3 us
    pallas_call x1, Pallas kernels, sp_gather(): pl.pallas_call(functools.partial(sp_gather_kernel, n_sp, n_tp), out_shape...  51.1 us
    pallas_call x2, Pallas kernels, tp_gather(): pl.pallas_call(functools.partial(tp_gather_kernel, n_tp), out_shape=jax.S...  44.5 us
    pallas_call x1, Pallas kernels, tp_scatter(): pl.pallas_call(functools.partial(tp_scatter_kernel, n_tp), out_shape=jax....  22.4 us
    unnamed x57, local copies, waits for them, and re-layouts  11.9 us
  transfers between devices with their start and end apart: 1, of which 0 were waited for; matrix products, arithmetic and copies ran while one was open for 9% of the time, Pallas kernels for 60%

commit v1 on v0

v1 whole, which is shorter than its diff:
```python
import functools
import math

import jax
import jax.numpy as jnp
import numpy as np
from jax import lax
from jax.experimental import pallas as pl
from jax.experimental.pallas import tpu as pltpu
from jax.sharding import PartitionSpec as P

GROUP = 256
NOPE = 64
ROPE = 32
VDIM = 64
HEAD = NOPE + ROPE
HALF = ROPE // 2
LANES = 128
RIM = 16
CHUNKS = 3
COLS = 4

norm_eps = 1e-06
rope_theta = 10000.0
bf16 = jnp.bfloat16
f32 = jnp.float32
MESH = pl.DeviceIdType.MESH
NT = (((1,), (1,)), ((), ()))


def up_to(n, m):
    return (n + m - 1) // m * m


def dot(a, b):
    return jnp.dot(a, b, preferred_element_type=f32)


def dot_nt(a, b):
    return lax.dot_general(a, b, NT, preferred_element_type=f32)


def remote(src, dst, send_sem, recv_sem, target):
    return pltpu.make_async_remote_copy(
        src_ref=src, dst_ref=dst, send_sem=send_sem, recv_sem=recv_sem, device_id=target, device_id_type=MESH
    )


def padded_transpose(w):
    rows, cols = w.shape
    r, c = up_to(rows, LANES), up_to(cols, LANES)
    w = w.astype(f32)
    if r > rows:
        w = jnp.concatenate([w, jnp.zeros((r - rows, cols), f32)], axis=0)
    if c > cols:
        w = jnp.concatenate([w, jnp.zeros((r, c - cols), f32)], axis=1)
    return w.T[:cols]


def mixer_kernel(
    n_sp,
    n_tp,
    x_hbm,
    wpool_hbm,
    wq_hbm,
    wkv_hbm,
    wkr_hbm,
    wqup_hbm,
    wkup_hbm,
    wvup_hbm,
    wop_hbm,
    woa_hbm,
    in_gain,
    pool_gain,
    qlat_gain,
    kvlat_gain,
    qh_gain,
    kh_gain,
    cos_q,
    sin_q,
    cos_k,
    sin_k,
    cos_b,
    sin_b,
    out_ref,
    x_own,
    wpool,
    wq_raw,
    wkv_raw,
    wkr_raw,
    wqup,
    wkup,
    wvup,
    wo,
    wo_p,
    wq_cat,
    wkv_cat,
    wq_t,
    wk_t,
    wv_pad,
    xg,
    qx,
    kv_mine,
    kvx,
    rope_own,
    kv_all,
    pool_ext,
    queries,
    keys_t,
    values,
    acc,
    act,
    act_p,
    f_out,
    f_in,
    ld_sem,
    a_far_send,
    a_near_send,
    a_relay_send,
    a_recv,
    kv_send,
    kv_recv,
    q_far_send,
    q_near_send,
    q_relay_send,
    q_recv,
    up_send,
    side_send,
    near_send,
    d_recv,
    p_send,
    p_recv,
    wo_send,
    wo_recv,
    act_send,
    act_recv,
    f_send,
    f_recv,
):
    me = lax.axis_index("tp")
    core, chip = lax.rem(me, 2), lax.div(me, 2)
    chips = n_tp // 2
    partner = me + 1 - 2 * core
    shard = lax.axis_index("sp")
    deep, side = lax.div(shard, 2), lax.rem(shard, 2)
    last_deep = n_sp // 2 - 1
    other = shard + 1 - 2 * side

    r, width = x_own.shape
    rows = r * n_tp
    half = r * chips
    qc = wq_raw.shape[1]
    kc = wkv_raw.shape[1]
    kvlat = kc * n_tp
    pc = wpool.shape[1]
    heads = wkup.shape[1] // NOPE
    hc = heads * VDIM
    rc = r // CHUNKS

    loads = {}

    def load(i, name, src, dst):
        loads[name] = pltpu.make_async_copy(src, dst, ld_sem.at[i])
        loads[name].start()

    load(0, "x", x_hbm, x_own)
    load(1, "wkv", wkv_hbm, wkv_raw)
    load(2, "wkr", wkr_hbm, wkr_raw)
    load(3, "wq", wq_hbm, wq_raw)
    load(4, "wpool", wpool_hbm, wpool)
    load(5, "wqup", wqup_hbm, wqup)
    load(6, "wkup", wkup_hbm, wkup)
    load(7, "wvup", wvup_hbm, wvup)
    load(8, "wop", wop_hbm, wo.at[pl.ds(0, pc), :])
    load(9, "woa", woa_hbm, wo.at[pl.ds(pc, hc), :])

    barrier = pltpu.get_barrier_semaphore()
    for step in range(1, n_tp):
        pl.semaphore_signal(
            barrier, inc=1, device_id={"tp": lax.rem(me + step, n_tp)}, device_id_type=MESH
        )
    greeted = n_tp - 1
    for gap in (-2, -1, 1, 2):
        there = shard + gap
        valid = (there >= 0) & (there < n_sp)

        @pl.when(valid)
        def _():
            pl.semaphore_signal(barrier, inc=1, device_id={"sp": there}, device_id_type=MESH)

        greeted = greeted + jnp.where(valid, 1, 0)
    pl.semaphore_wait(barrier, greeted)

    def place(k, c):
        return 2 * k + c

    def behind(step):
        return lax.rem(chip + chips - step, chips)

    def ahead(step):
        return lax.rem(chip + step, chips)

    def rows_at(g, off, count):
        return pl.ds(pl.multiple_of(g * r + off, 16), count)

    def arrived(ref, sem):
        remote(ref, ref, a_near_send.at[0], sem, {"tp": partner}).wait_recv()

    sends = []
    loads["x"].wait()
    for c in range(CHUNKS):
        at = pl.ds(c * rc, rc)
        xf = x_own[at, :].astype(f32)
        factor = lax.rsqrt(jnp.mean(xf * xf, axis=1, keepdims=True) + norm_eps)
        xg[me, at, :] = (xf * factor * in_gain[...]).astype(bf16)
        own = xg.at[me, at, :]
        for step in range(1, chips):
            copy = remote(
                own, own, a_far_send.at[step - 1, c], a_recv.at[me, c], {"tp": place(ahead(step), core)}
            )
            copy.start()
            sends.append(copy)
    for c in range(CHUNKS):
        own = xg.at[me, pl.ds(c * rc, rc), :]
        copy = remote(own, own, a_near_send.at[c], a_recv.at[me, c], {"tp": partner})
        copy.start()
        sends.append(copy)

    loads["wkv"].wait()
    loads["wkr"].wait()
    wkv_cat[...] = jnp.zeros_like(wkv_cat)
    wkv_cat[:, :kc] = wkv_raw[...]
    wkv_cat[:, LANES : LANES + ROPE] = wkr_raw[...]
    loads["wq"].wait()
    wq_cat[...] = jnp.zeros_like(wq_cat)
    wq_cat[:, :qc] = wq_raw[...]
    loads["wpool"].wait()

    def project(k, c, off, count, same_core):
        g = place(k, c)
        xs = xg[g, pl.ds(off, count), :]
        at = rows_at(g, off, count)
        both = dot(xs, wkv_cat[...])
        kv_mine[c, k, pl.ds(off, count), :] = both[:, :kc].astype(bf16)
        if same_core:
            shared = both[:, LANES : 2 * LANES].astype(bf16).astype(f32)
            rope_own[pl.ds(pl.multiple_of(k * r + off, 8), count), :] = shared
        qx[me, at, :] = dot(xs, wq_cat[...]).astype(bf16)
        at_ext = pl.ds(pl.multiple_of(g * r + off + RIM, 16), count)
        pool_ext[at_ext, :] = dot(xs, wpool[...]).astype(bf16)

    project(chip, core, 0, r, True)
    for c in range(CHUNKS):
        arrived(xg.at[partner, pl.ds(c * rc, rc), :], a_recv.at[partner, c])
    project(chip, 1 - core, 0, r, False)

    loads["wqup"].wait()
    for src in range(n_tp):
        part = wqup[src * qc : (src + 1) * qc, :].astype(f32) * qlat_gain[src * qc : (src + 1) * qc, :]
        wq_t[src] = padded_transpose(part).astype(bf16)
    loads["wkup"].wait()
    wk_t[...] = padded_transpose(wkup[...]).astype(bf16)
    loads["wvup"].wait()
    wv_pad[...] = jnp.zeros_like(wv_pad)
    for h in range(heads):
        wv_pad[:, h * LANES : h * LANES + VDIM] = (
            wvup[...].astype(f32)[:, h * VDIM : (h + 1) * VDIM].astype(bf16)
        )
    keys_t[:, HEAD:, :] = jnp.zeros((heads, LANES - HEAD, rows), bf16)
    acc[...] = jnp.zeros_like(acc)

    loads["wop"].wait()
    loads["woa"].wait()
    wo_copy = remote(wo, wo_p, wo_send, wo_recv, {"tp": partner})
    wo_copy.start()

    for c in range(CHUNKS):
        at = pl.ds(c * rc, rc)
        for step in range(1, chips):
            g = place(behind(step), core)
            block = xg.at[g, at, :]
            arrived(block, a_recv.at[g, c])
            copy = remote(block, block, a_relay_send.at[step - 1, c], a_recv.at[g, c], {"tp": partner})
            copy.start()
            sends.append(copy)
        for step in range(1, chips):
            project(behind(step), core, c * rc, rc, True)
        for step in range(1, chips):
            g = place(behind(step), 1 - core)
            arrived(xg.at[g, at, :], a_recv.at[g, c])
            project(behind(step), 1 - core, c * rc, rc, False)

    for step in range(1, n_tp):
        there = lax.rem(me + step, n_tp)
        copy = remote(
            kv_mine.at[lax.rem(there, 2)], kvx.at[me], kv_send.at[step - 1], kv_recv.at[me], {"tp": there}
        )
        copy.start()
        sends.append(copy)
    own_q = qx.at[me]
    for step in range(1, chips):
        copy = remote(own_q, own_q, q_far_send.at[step - 1], q_recv.at[me], {"tp": place(ahead(step), core)})
        copy.start()
        sends.append(copy)
    copy = remote(own_q, own_q, q_near_send, q_recv.at[me], {"tp": partner})
    copy.start()
    sends.append(copy)

    rim_copy = remote(
        pool_ext.at[pl.ds(rows, RIM), :], pool_ext.at[pl.ds(0, RIM), :], p_send, p_recv, {"sp": shard + 1}
    )

    @pl.when(shard < n_sp - 1)
    def _():
        rim_copy.start()

    @pl.when(shard == 0)
    def _():
        pool_ext[pl.ds(0, RIM), :] = jnp.zeros((RIM, pc), bf16)

    kvx[me] = kv_mine[core]
    for step in range(1, n_tp):
        source = lax.rem(me + step, n_tp)
        arrived(kvx.at[source], kv_recv.at[source])
    lat = jnp.concatenate([kvx[i].reshape(half, kc).astype(f32) for i in range(n_tp)], axis=1)
    factor = lax.rsqrt(jnp.mean(lat * lat, axis=1, keepdims=True) + norm_eps)
    kv_all[shard, core, pl.ds(0, half), :] = (lat * factor * kvlat_gain[...]).astype(bf16)
    kv_all[shard, core, pl.ds(half, ROPE), pl.ds(0, half)] = rope_own[...].T[:ROPE].astype(bf16)

    def piece(block, h):
        return kv_all.at[block, h]

    def onward(block):
        return remote(
            piece(block, core), piece(block, core), up_send.at[block], d_recv.at[block, core], {"sp": shard + 2}
        )

    def across(block):
        return remote(
            piece(block, core), piece(block, core), side_send.at[block], d_recv.at[block, core], {"sp": other}
        )

    def near(block):
        return remote(
            piece(block, core), piece(block, core), near_send.at[block], d_recv.at[block, core], {"tp": partner}
        )

    @pl.when(deep < last_deep)
    def _():
        onward(shard).start()

    @pl.when(side == 0)
    def _():
        across(shard).start()

    near(shard).start()

    for step in range(1, chips):
        g = place(behind(step), core)
        arrived(qx.at[g], q_recv.at[g])
        copy = remote(qx.at[g], qx.at[g], q_relay_send.at[step - 1], q_recv.at[g], {"tp": partner})
        copy.start()
        sends.append(copy)
    for k in range(chips):
        g = place(k, 1 - core)
        arrived(qx.at[g], q_recv.at[g])

    score_scale = HEAD ** (-0.5) * math.log2(math.e)
    q_tile = 2 * r

    def table(cos_ref, sin_ref, block, at):
        ca, sa = cos_ref[:, at], sin_ref[:, at]
        cb, sb = cos_b[block], sin_b[block]
        return ca * cb - sa * sb, sa * cb + ca * sb

    def make_queries(i, _):
        at = pl.ds(pl.multiple_of(i * LANES, LANES), LANES)
        raw = None
        squares = None
        ones = jnp.ones((8, qx.shape[2]), bf16)
        for src in range(n_tp):
            part = qx[src, at, :]
            term = dot_nt(wq_t[src], part)
            raw = term if raw is None else raw + term
            pf = part.astype(f32)
            term = dot_nt(ones, (pf * pf).astype(bf16))
            squares = term if squares is None else squares + term
        eps = norm_eps * (squares[:1] * (1.0 / (qc * n_tp)) + norm_eps)
        cosine, sine = table(cos_q, sin_q, shard, at)
        for h in range(heads):
            x = raw[h * HEAD : (h + 1) * HEAD]
            factor = lax.rsqrt(jnp.sum(x * x, axis=0, keepdims=True) * (1.0 / HEAD) + eps) * score_scale
            y = x * factor * qh_gain[...]
            low, high = y[NOPE : NOPE + HALF], y[NOPE + HALF :]
            full = jnp.concatenate(
                [
                    y[:NOPE] * kh_gain[:NOPE, :],
                    low * cosine - high * sine,
                    high * cosine + low * sine,
                    jnp.zeros((LANES - HEAD, LANES), f32),
                ],
                axis=0,
            )
            queries[h, at, :] = full.T.astype(bf16)
        return 0

    lax.fori_loop(0, rows // LANES, make_queries, 0)

    lane = lax.broadcasted_iota(jnp.int32, (half, LANES), 1)

    def prepare(block):
        for c in range(2):
            at = pl.ds(c * half, half)
            lat = kv_all[block, c, pl.ds(0, half), :]
            shared = kv_all[block, c, pl.ds(half, ROPE), pl.ds(0, half)].astype(f32)
            shared_sq = jnp.sum(shared * shared, axis=0, keepdims=True)
            cosine, sine = table(cos_k, sin_k, block, at)
            gained = shared * kh_gain[NOPE:, :]
            low, high = gained[:HALF], gained[HALF:]
            turned = jnp.concatenate([low * cosine - high * sine, high * cosine + low * sine], axis=0)
            plain = dot_nt(wk_t[...], lat)
            value = dot(lat, wv_pad[...])
            for h in range(heads):
                x = plain[h * NOPE : (h + 1) * NOPE]
                total = jnp.sum(x * x, axis=0, keepdims=True) + shared_sq
                factor = lax.rsqrt(total * (1.0 / HEAD) + norm_eps)
                keys_t[h, :NOPE, at] = (x * factor).astype(bf16)
                keys_t[h, NOPE:HEAD, at] = (turned * factor).astype(bf16)
                v = jnp.where(lane == VDIM, 1.0, value[:, h * LANES : (h + 1) * LANES])
                values[h, at, :] = v.astype(bf16)

    key_tile = math.gcd(half, 384)

    def accumulate(i, masked):
        at = pl.ds(pl.multiple_of(i * q_tile, q_tile), q_tile)
        for h in range(heads):
            q = queries[h, at, :]
            total = acc[h, at, :]
            for j in range(rows // key_tile):
                cols = pl.ds(j * key_tile, key_tile)
                weights = jnp.exp2(dot(q, keys_t[h, :, cols]))
                if masked:
                    q_pos = i * q_tile + lax.broadcasted_iota(jnp.int32, weights.shape, 0)
                    col = (j * key_tile) % half + lax.broadcasted_iota(jnp.int32, weights.shape, 1)
                    k_pos = col + ((j * key_tile) // half) * r
                    for k in range(1, chips):
                        k_pos = k_pos + jnp.where(col >= k * r, r, 0)
                    weights = jnp.where(k_pos <= q_pos, weights, 0.0)
                total = total + dot(weights.astype(bf16), values[h, cols, :])
            acc[h, at, :] = total

    def all_rows(masked):
        def one(i, _):
            accumulate(i, masked)
            return 0

        lax.fori_loop(0, chips, one, 0)

    def block_of(j):
        odd = lax.rem(j, 2)
        jj = jnp.where(side == 1, j, j - 1 + 2 * odd)
        return shard - jj, 1 - lax.rem(jj, 2)

    def forward(j):
        block, mine = block_of(j)
        arrived(piece(block, core), d_recv.at[block, core])

        @pl.when((mine == 1) & (deep < last_deep))
        def _():
            onward(block).start()

        @pl.when(mine == 1)
        def _():
            across(block).start()

        near(block).start()

    def ready(j):
        block, _ = block_of(j)
        arrived(piece(block, 1 - core), d_recv.at[block, 1 - core])
        prepare(block)

    def one_block(j, _):
        forward(j)

        @pl.when(j > 1)
        def _():
            ready(j - 1)
            all_rows(False)

        return 0

    @pl.when(shard > 0)
    def _():
        arrived(pool_ext.at[pl.ds(0, RIM), :], p_recv)

    def pool(i, _):
        base = pl.multiple_of(i * LANES, LANES)
        ext = pool_ext[pl.ds(base, LANES + RIM), :].astype(f32)
        channel = me * pc + lax.broadcasted_iota(jnp.int32, (LANES, pc), 1)
        window = jnp.left_shift(jnp.int32(2), lax.div(channel, GROUP))
        total = ext
        chosen = None
        for level in range(4):
            total = total + pltpu.roll(total, 1 << level, 0)
            if chosen is None:
                chosen = total[RIM:]
            else:
                chosen = jnp.where(window >= (2 << level), total[RIM:], chosen)
        position = shard * rows + base + lax.broadcasted_iota(jnp.int32, (LANES, pc), 0)
        divisor = jnp.minimum(position + 1, window).astype(f32)
        pooled = (chosen / divisor - ext[RIM:]) * pool_gain[...]
        act[pl.ds(base, LANES), :pc] = pooled.astype(bf16)
        return 0

    lax.fori_loop(0, rows // LANES, pool, 0)

    lax.fori_loop(1, shard + 1, one_block, 0)

    arrived(piece(shard, 1 - core), d_recv.at[shard, 1 - core])
    prepare(shard)
    all_rows(True)

    @pl.when(shard > 0)
    def _():
        ready(shard)

        def one(step, _):
            accumulate(lax.rem(chip + step, chips), False)
            return 0

        lax.fori_loop(1, chips, one, 0)

    def finish(k):
        at = pl.ds(pl.multiple_of(k * q_tile, q_tile), q_tile)
        parts = []
        for h in range(heads):
            a = acc[h, at, :]
            parts.append(a[:, :VDIM] / a[:, VDIM : VDIM + 1])
        act[at, pc:] = jnp.concatenate(parts, axis=1).astype(bf16)
        copy = remote(
            act.at[rows_at(place(k, 1 - core), 0, r), :], act_p.at[k], act_send.at[k], act_recv.at[k], {"tp": partner}
        )
        copy.start()
        sends.append(copy)

    cw = width // COLS

    def product(k, n):
        cols = pl.ds(n * cw, cw)
        mine = act[rows_at(place(k, core), 0, r), :]
        return dot(mine, wo[:, cols]) + dot(act_p[k], wo_p[:, cols])

    for step in range(1, chips):
        finish(ahead(step))
    arrived(wo_p, wo_recv)
    for step in range(1, chips):
        k = ahead(step)
        arrived(act_p.at[k], act_recv.at[k])
        for n in range(COLS):
            f_out[step - 1, n] = product(k, n).astype(bf16)
            copy = remote(
                f_out.at[step - 1, n],
                f_in.at[step - 1, n],
                f_send.at[step - 1, n],
                f_recv.at[step - 1, n],
                {"tp": place(k, core)},
            )
            copy.start()
            sends.append(copy)

    @pl.when(shard > 0)
    def _():
        accumulate(chip, False)

    finish(chip)
    arrived(act_p.at[chip], act_recv.at[chip])
    for n in range(COLS):
        total = product(chip, n)
        for step in range(1, chips):
            arrived(f_in.at[step - 1, n], f_recv.at[step - 1, n])
            total = total + f_in[step - 1, n].astype(f32)
        out_ref[:, n * cw : (n + 1) * cw] = total.astype(bf16)

    for copy in sends:
        copy.wait_send()
    wo_copy.wait_send()

    @pl.when(shard < n_sp - 1)
    def _():
        rim_copy.wait_send()

    def drain(j, _):
        block = shard - j
        near(block).wait_send()

        @pl.when((lax.rem(j, 2) == 0) & (deep < last_deep))
        def _():
            onward(block).wait_send()

        @pl.when((lax.rem(j, 2) == 0) & ((j > 0) | (side == 0)))
        def _():
            across(block).wait_send()

        return 0

    lax.fori_loop(0, shard + 1, drain, 0)


def tables(n_sp, n_tp, rows):
    frequency = np.float32(rope_theta) ** (-np.arange(0, ROPE, 2, dtype=np.float32) / np.float32(ROPE))
    r = rows // n_tp

    def make(positions):
        angles = frequency.astype(np.float32)[:, None] * positions.astype(np.float32)[None, :]
        angles = angles.astype(np.float64)
        return np.cos(angles).astype(np.float32), np.sin(angles).astype(np.float32)

    natural = np.arange(rows)
    split = natural.reshape(n_tp // 2, 2, r).transpose(1, 0, 2).reshape(-1)
    blocks = make(np.arange(n_sp) * rows)
    columns = [np.ascontiguousarray(t.T)[:, :, None] for t in blocks]
    return [*make(natural), *make(split), *columns]


def local(
    activations,
    in_gain,
    w_pool_in,
    pool_gain,
    w_qlat,
    w_kvlat,
    w_krope,
    qlat_gain,
    kvlat_gain,
    w_qup,
    w_kup,
    w_vup,
    qhead_gain,
    khead_gain,
    w_out_pool,
    w_out_attn,
):
    n_sp, n_tp = lax.axis_size("sp"), lax.axis_size("tp")
    r, width = activations.shape
    rows, chips = r * n_tp, n_tp // 2
    half = r * chips
    others = max(1, chips - 1)
    qc, kc, pc = w_qlat.shape[1], w_kvlat.shape[1], w_pool_in.shape[1]
    heads = w_kup.shape[1] // NOPE
    kvlat = w_kup.shape[0]
    hc = heads * VDIM
    qp = up_to(qc, LANES)
    vm = pl.BlockSpec(memory_space=pltpu.VMEM)
    hbm = pl.BlockSpec(memory_space=pl.ANY)
    scratch = [
        ((r, width), bf16),
        ((width, pc), bf16),
        ((width, qc), bf16),
        ((width, kc), bf16),
        (w_krope.shape, bf16),
        (w_qup.shape, bf16),
        (w_kup.shape, bf16),
        (w_vup.shape, bf16),
        ((pc + hc, width), bf16),
        ((pc + hc, width), bf16),
        ((width, qp), bf16),
        ((width, 2 * LANES), bf16),
        ((n_tp, heads * HEAD, qp), bf16),
        ((heads * NOPE, kvlat), bf16),
        ((kvlat, heads * LANES), bf16),
        ((n_tp, r, width), bf16),
        ((n_tp, rows, qp), bf16),
        ((2, chips, r, kc), bf16),
        ((n_tp, chips, r, kc), bf16),
        ((half, LANES), f32),
        ((n_sp, 2, half + ROPE, kvlat), bf16),
        ((rows + RIM, pc), bf16),
        ((heads, rows, LANES), bf16),
        ((heads, LANES, rows), bf16),
        ((heads, rows, LANES), bf16),
        ((heads, rows, LANES), f32),
        ((rows, pc + hc), bf16),
        ((chips, r, pc + hc), bf16),
        ((others, COLS, r, width // COLS), bf16),
        ((others, COLS, r, width // COLS), bf16),
    ]
    dma = pltpu.SemaphoreType.DMA
    sems = [
        (10,),
        (others, CHUNKS),
        (CHUNKS,),
        (others, CHUNKS),
        (n_tp, CHUNKS),
        (n_tp,),
        (n_tp,),
        (others,),
        None,
        (others,),
        (n_tp,),
        (n_sp,),
        (n_sp,),
        (n_sp,),
        (n_sp, 2),
        None,
        None,
        None,
        None,
        (chips,),
        (chips,),
        (others, COLS),
        (others, COLS),
    ]
    small = [
        in_gain.reshape(1, -1),
        pool_gain.reshape(1, -1),
        qlat_gain.reshape(-1, 1),
        kvlat_gain.reshape(1, -1),
        qhead_gain.reshape(-1, 1),
        khead_gain.reshape(-1, 1),
    ] + [jnp.asarray(t) for t in tables(n_sp, n_tp, rows)]
    return pl.pallas_call(
        functools.partial(mixer_kernel, n_sp, n_tp),
        out_shape=jax.ShapeDtypeStruct((r, width), bf16),
        in_specs=[hbm] * 10 + [vm] * len(small),
        out_specs=vm,
        scratch_shapes=[pltpu.VMEM(s, d) for s, d in scratch] + [dma if s is None else dma(s) for s in sems],
        compiler_params=pltpu.CompilerParams(
            collective_id=0, has_side_effects=True, vmem_limit_bytes=67_043_328
        ),
    )(
        activations,
        w_pool_in,
        w_qlat,
        w_kvlat,
        w_krope,
        w_qup,
        w_kup,
        w_vup,
        w_out_pool,
        w_out_attn,
        *small,
    )


def solution(mesh):
    placed = (
        P(("sp", "tp"), None),
        P(),
        P(None, "tp"),
        P("tp"),
        P(None, "tp"),
        P(None, "tp"),
        P(),
        P(),
        P(),
        P(None, "tp"),
        P(None, "tp"),
        P(None, "tp"),
        P(),
        P(),
        P("tp", None),
        P("tp", None),
    )
    return jax.shard_map(
        local, mesh=mesh, in_specs=placed, out_specs=P(("sp", "tp"), None), check_vma=False
    )
```

time: 214 us -> 131 us (0.61)
  Pallas kernels: 175 us -> 119 us
  matrix products: 10.5 us -> 0 us
  other arithmetic: 10.4 us -> 0 us
  local copies, waits for them, and re-layouts: 14.8 us -> 9.71 us
    pallas_call x5 -> x1, Pallas kernels: 175 us -> 119 us  [local(): pl.pallas_call(functools.partial(mixer_kernel, n_sp, n_tp), out_shape=jax...]
    dot_general x6 -> x0, matrix products: 10.5 us -> none  [the longest x1 3.04 us: local(): jnp.dot(normed, krope_pad, preferred_element_type=f32).astype(bf16)]
    unnamed x57 -> x5, local copies, waits for them, and re-layouts: 11.9 us -> 5.3 us
    reshape x2 -> x3, local copies, waits for them, and re-layouts: 0.01 us -> 4.41 us  [the longest x1 1.6 us: local(): qlat_gain.reshape(-1, 1)]
    concatenate x4 -> x0, other arithmetic: 2.98 us -> none  [the longest x2 1.42 us: make(): jnp.concatenate([jnp.zeros((count, NOPE), f32), sine, sine, jnp.zeros((co...]
    convert_element_type x4 -> x0, other arithmetic: 2.85 us -> none  [the longest x1 2.76 us: local(): normed = row_norm(own_input, in_gain).astype(bf16)]
    reduce_sum x1 -> x0, other arithmetic: 2.58 us -> none  [row_norm(): jnp.mean(as_float * as_float, axis=-1, keepdims=True) + norm_eps]
    squeeze x1 -> x0, local copies, waits for them, and re-layouts: 2.55 us -> none  [local(): latents[i, :, :q_width]]
  transfers between devices with their start and end apart: 1 -> 0, of which waited for: 0 -> 0; matrix products, arithmetic and copies ran while one was open for 9% -> 0% of each run, Pallas kernels for 60% -> 0%
where the time goes in v1:
time: 131 us; the launch traced here: 129 us
  Pallas kernels  119 us (91%)
  local copies, waits for them, and re-layouts  9.71 us (7%)
    pallas_call x1, Pallas kernels, local(): pl.pallas_call(functools.partial(mixer_kernel, n_sp, n_tp), out_shape=jax...  119 us
    unnamed x5, local copies, waits for them, and re-layouts  5.3 us

profile of v1, /device:TPU:28, one launch (start us, length us, event | category | flops | bytes accessed | tf_op | source)
XLA Modules:
  0.0 128.8 jit_solution(15159302644465896138)
XLA Ops:
  0.0 0.0 copy-start
  0.0 1.4 %copy.30.qh_gain = f32[96,1]{1,0:T(8,128)} copy(f32[96,1]{0,1:T(1,128)} %bitcast.8) | data formatting | bytes 768 | tf_op jit(solution)/shard_map/reshape | solution.py:719
  1.4 1.4 %copy.31.kh_gain = f32[96,1]{1,0:T(8,128)} copy(f32[96,1]{0,1:T(1,128)} %bitcast.9) | data formatting | bytes 768 | tf_op jit(solution)/shard_map/reshape | solution.py:720
  2.8 1.6 %reshape.24.qlat_gain = f32[768,1]{1,0:T(8,128)} reshape(f32[768]{0:T(1024)} %param.29) | data formatting | bytes 6144 | tf_op jit(solution)/shard_map/reshape | solution.py:717
  4.4 1.9 %copy.28.wkr_hbm = bf16[2048,32]{1,0:T(8,128)(2,1)} copy(bf16[2048,32]{0,1:T(8,128)(2,1)} %param.28) | data formatting | bytes 262144 | tf_op args[6]
  6.3 0.0 copy-done
  6.3 1.3 %copy.27.wq_hbm = bf16[2048,192]{1,0:T(8,128)(2,1)} copy(bf16[2048,192]{0,1:T(8,128)(2,1)S(1)} %copy-done) | data formatting | bytes 1572864 | tf_op args[4]
  7.6 119.1 %shard_map.208 = bf16[192,2048]{1,0:T(8,128)(2,1)} custom-call(bf16[192,2048]{1,0:T(8,128)(2,1)} %x_hbm.1, bf16[2048,256]{1,0:T(8,128)(2,1)} %wpool_hbm.1, bf16[2048,192]{1,0:T(8,128)(2,1)} %copy.27.wq_hbm, bf16[2048,128]{1,0:T(8,128)(2,1)} %wkv_hbm.1, bf16[2048,32]{1,0:T(8,128)(2,1)} %copy.28.wkr_hbm, bf16[768,384]{1,0:T(8,128)(2,1)} %wqup_hbm.1, ...), custom_call_target="tpu_custom_call" | custom-call | tf_op jit(solution)/shard_map/pallas_call | solution.py:722
  126.7 2.1 %copy.33 = bf16[192,2048]{1,0:T(8,128)(2,1)} copy(bf16[192,2048]{1,0:T(8,128)(2,1)} %shard_map.208) | data formatting | bytes 1572864
Async XLA Ops:
  0.0 6.3 %copy-start = (bf16[2048,192]{0,1:T(8,128)(2,1)S(1)}, bf16[2048,192]{0,1:T(8,128)(2,1)}, u32[]{:S(2)}) copy-start(bf16[2048,192]{0,1:T(8,128)(2,1)} %param.26) | copy-start | bytes 2359300

commit v2 on v1

--- a/solution.py
+++ b/solution.py
@@ -19,6 +19,8 @@
 RIM = 16
 CHUNKS = 3
 COLS = 4
+VMEM_MOST = 67_043_328
+SPARE = 6 * 1024 * 1024
 
 norm_eps = 1e-06
 rope_theta = 10000.0
@@ -57,9 +59,18 @@
     return w.T[:cols]
 
 
+def column(row):
+    count = row.shape[1]
+    wide = up_to(count, LANES)
+    if wide > count:
+        row = jnp.concatenate([row, jnp.zeros((1, wide - count), f32)], axis=1)
+    return jnp.broadcast_to(row, (LANES, wide)).T[:count]
+
+
 def mixer_kernel(
     n_sp,
     n_tp,
+    keep,
     x_hbm,
     wpool_hbm,
     wq_hbm,
@@ -70,6 +81,19 @@
     wvup_hbm,
     wop_hbm,
     woa_hbm,
+    in_gain_hbm,
+    pool_gain_hbm,
+    qlat_gain_hbm,
+    kvlat_gain_hbm,
+    qh_gain_hbm,
+    kh_gain_hbm,
+    cos_q_hbm,
+    sin_q_hbm,
+    cos_k_hbm,
+    sin_k_hbm,
+    cos_b_hbm,
+    sin_b_hbm,
+    out_ref,
     in_gain,
     pool_gain,
     qlat_gain,
@@ -82,7 +106,6 @@
     sin_k,
     cos_b,
     sin_b,
-    out_ref,
     x_own,
     wpool,
     wq_raw,
@@ -98,6 +121,8 @@
     wq_t,
     wk_t,
     wv_pad,
+    gain_q,
+    gain_k,
     xg,
     qx,
     kv_mine,
@@ -149,7 +174,7 @@
     r, width = x_own.shape
     rows = r * n_tp
     half = r * chips
-    qc = wq_raw.shape[1]
+    qc = wq_raw.shape[0]
     kc = wkv_raw.shape[1]
     kvlat = kc * n_tp
     pc = wpool.shape[1]
@@ -164,6 +189,7 @@
         loads[name].start()
 
     load(0, "x", x_hbm, x_own)
+    load(10, "in_gain", in_gain_hbm, in_gain)
     load(1, "wkv", wkv_hbm, wkv_raw)
     load(2, "wkr", wkr_hbm, wkr_raw)
     load(3, "wq", wq_hbm, wq_raw)
@@ -173,6 +199,21 @@
     load(7, "wvup", wvup_hbm, wvup)
     load(8, "wop", wop_hbm, wo.at[pl.ds(0, pc), :])
     load(9, "woa", woa_hbm, wo.at[pl.ds(pc, hc), :])
+    small = {
+        "pool_gain": (pool_gain_hbm, pool_gain),
+        "qlat_gain": (qlat_gain_hbm, qlat_gain),
+        "kvlat_gain": (kvlat_gain_hbm, kvlat_gain),
+        "qh_gain": (qh_gain_hbm, qh_gain),
+        "kh_gain": (kh_gain_hbm, kh_gain),
+        "cos_q": (cos_q_hbm, cos_q),
+        "sin_q": (sin_q_hbm, sin_q),
+        "cos_k": (cos_k_hbm, cos_k),
+        "sin_k": (sin_k_hbm, sin_k),
+        "cos_b": (cos_b_hbm, cos_b),
+        "sin_b": (sin_b_hbm, sin_b),
+    }
+    for i, (name, pair) in enumerate(small.items()):
+        load(11 + i, name, *pair)
 
     barrier = pltpu.get_barrier_semaphore()
     for step in range(1, n_tp):
@@ -208,6 +249,7 @@
 
     sends = []
     loads["x"].wait()
+    loads["in_gain"].wait()
     for c in range(CHUNKS):
         at = pl.ds(c * rc, rc)
         xf = x_own[at, :].astype(f32)
@@ -228,12 +270,10 @@
 
     loads["wkv"].wait()
     loads["wkr"].wait()
-    wkv_cat[...] = jnp.zeros_like(wkv_cat)
     wkv_cat[:, :kc] = wkv_raw[...]
-    wkv_cat[:, LANES : LANES + ROPE] = wkr_raw[...]
+    wkv_cat[:, LANES:] = padded_transpose(wkr_raw[...]).astype(bf16)
     loads["wq"].wait()
-    wq_cat[...] = jnp.zeros_like(wq_cat)
-    wq_cat[:, :qc] = wq_raw[...]
+    wq_cat[...] = padded_transpose(wq_raw[...]).astype(bf16)
     loads["wpool"].wait()
 
     def project(k, c, off, count, same_core):
@@ -255,8 +295,15 @@
     project(chip, 1 - core, 0, r, False)
 
     loads["wqup"].wait()
+    for name in small:
+        loads[name].wait()
+    lat_rows = qlat_gain[...]
+    lat_gain = jnp.concatenate([column(lat_rows[i : i + 1]) for i in range(lat_rows.shape[0])], axis=0)
+    gain_q[...] = column(qh_gain[...])
+    gain_k[...] = column(kh_gain[...])
     for src in range(n_tp):
-        part = wqup[src * qc : (src + 1) * qc, :].astype(f32) * qlat_gain[src * qc : (src + 1) * qc, :]
+        span = slice(src * qc, (src + 1) * qc)
+        part = wqup[span, :].astype(f32) * lat_gain[span, :1]
         wq_t[src] = padded_transpose(part).astype(bf16)
     loads["wkup"].wait()
     wk_t[...] = padded_transpose(wkup[...]).astype(bf16)
@@ -266,7 +313,6 @@
         wv_pad[:, h * LANES : h * LANES + VDIM] = (
             wvup[...].astype(f32)[:, h * VDIM : (h + 1) * VDIM].astype(bf16)
         )
-    keys_t[:, HEAD:, :] = jnp.zeros((heads, LANES - HEAD, rows), bf16)
     acc[...] = jnp.zeros_like(acc)
 
     loads["wop"].wait()
@@ -355,16 +401,6 @@
 
     near(shard).start()
 
-    for step in range(1, chips):
-        g = place(behind(step), core)
-        arrived(qx.at[g], q_recv.at[g])
-        copy = remote(qx.at[g], qx.at[g], q_relay_send.at[step - 1], q_recv.at[g], {"tp": partner})
-        copy.start()
-        sends.append(copy)
-    for k in range(chips):
-        g = place(k, 1 - core)
-        arrived(qx.at[g], q_recv.at[g])
-
     score_scale = HEAD ** (-0.5) * math.log2(math.e)
     q_tile = 2 * r
 
@@ -374,7 +410,7 @@
         return ca * cb - sa * sb, sa * cb + ca * sb
 
     def make_queries(i, _):
-        at = pl.ds(pl.multiple_of(i * LANES, LANES), LANES)
+        at = pl.ds(pl.multiple_of(i * half, half), half)
         raw = None
         squares = None
         ones = jnp.ones((8, qx.shape[2]), bf16)
@@ -390,32 +426,32 @@
         for h in range(heads):
             x = raw[h * HEAD : (h + 1) * HEAD]
             factor = lax.rsqrt(jnp.sum(x * x, axis=0, keepdims=True) * (1.0 / HEAD) + eps) * score_scale
-            y = x * factor * qh_gain[...]
+            y = x * factor * gain_q[:, :1]
             low, high = y[NOPE : NOPE + HALF], y[NOPE + HALF :]
             full = jnp.concatenate(
                 [
-                    y[:NOPE] * kh_gain[:NOPE, :],
+                    y[:NOPE] * gain_k[:NOPE, :1],
                     low * cosine - high * sine,
                     high * cosine + low * sine,
-                    jnp.zeros((LANES - HEAD, LANES), f32),
+                    jnp.zeros((LANES - HEAD, half), f32),
                 ],
                 axis=0,
             )
             queries[h, at, :] = full.T.astype(bf16)
         return 0
 
-    lax.fori_loop(0, rows // LANES, make_queries, 0)
 
     lane = lax.broadcasted_iota(jnp.int32, (half, LANES), 1)
 
     def prepare(block):
+        slot = block if keep else 0
         for c in range(2):
             at = pl.ds(c * half, half)
             lat = kv_all[block, c, pl.ds(0, half), :]
             shared = kv_all[block, c, pl.ds(half, ROPE), pl.ds(0, half)].astype(f32)
             shared_sq = jnp.sum(shared * shared, axis=0, keepdims=True)
             cosine, sine = table(cos_k, sin_k, block, at)
-            gained = shared * kh_gain[NOPE:, :]
+            gained = shared * gain_k[NOPE:, :1]
             low, high = gained[:HALF], gained[HALF:]
             turned = jnp.concatenate([low * cosine - high * sine, high * cosine + low * sine], axis=0)
             plain = dot_nt(wk_t[...], lat)
@@ -424,21 +460,23 @@
                 x = plain[h * NOPE : (h + 1) * NOPE]
                 total = jnp.sum(x * x, axis=0, keepdims=True) + shared_sq
                 factor = lax.rsqrt(total * (1.0 / HEAD) + norm_eps)
-                keys_t[h, :NOPE, at] = (x * factor).astype(bf16)
-                keys_t[h, NOPE:HEAD, at] = (turned * factor).astype(bf16)
+                keys_t[slot, h, :NOPE, at] = (x * factor).astype(bf16)
+                keys_t[slot, h, NOPE:HEAD, at] = (turned * factor).astype(bf16)
+                keys_t[slot, h, HEAD:, at] = jnp.zeros((LANES - HEAD, half), bf16)
                 v = jnp.where(lane == VDIM, 1.0, value[:, h * LANES : (h + 1) * LANES])
-                values[h, at, :] = v.astype(bf16)
+                values[slot, h, at, :] = v.astype(bf16)
 
     key_tile = math.gcd(half, 384)
 
-    def accumulate(i, masked):
+    def accumulate(block, i, masked):
+        slot = block if keep else 0
         at = pl.ds(pl.multiple_of(i * q_tile, q_tile), q_tile)
         for h in range(heads):
             q = queries[h, at, :]
             total = acc[h, at, :]
             for j in range(rows // key_tile):
                 cols = pl.ds(j * key_tile, key_tile)
-                weights = jnp.exp2(dot(q, keys_t[h, :, cols]))
+                weights = jnp.exp2(dot(q, keys_t[slot, h, :, cols]))
                 if masked:
                     q_pos = i * q_tile + lax.broadcasted_iota(jnp.int32, weights.shape, 0)
                     col = (j * key_tile) % half + lax.broadcasted_iota(jnp.int32, weights.shape, 1)
@@ -446,49 +484,52 @@
                     for k in range(1, chips):
                         k_pos = k_pos + jnp.where(col >= k * r, r, 0)
                     weights = jnp.where(k_pos <= q_pos, weights, 0.0)
-                total = total + dot(weights.astype(bf16), values[h, cols, :])
+                total = total + dot(weights.astype(bf16), values[slot, h, cols, :])
             acc[h, at, :] = total
 
-    def all_rows(masked):
-        def one(i, _):
-            accumulate(i, masked)
+    def far_rows(block, masked):
+        def one(step, _):
+            accumulate(block, lax.rem(chip + step, chips), masked)
             return 0
 
-        lax.fori_loop(0, chips, one, 0)
-
-    def block_of(j):
-        odd = lax.rem(j, 2)
-        jj = jnp.where(side == 1, j, j - 1 + 2 * odd)
-        return shard - jj, 1 - lax.rem(jj, 2)
-
-    def forward(j):
-        block, mine = block_of(j)
-        arrived(piece(block, core), d_recv.at[block, core])
-
-        @pl.when((mine == 1) & (deep < last_deep))
+        lax.fori_loop(1, chips, one, 0)
+
+    def early_rows(block, masked):
+        far_rows(block, masked)
+        if not keep:
+            accumulate(block, chip, masked)
+
+    def z_block(e):
+        return shard - 2 * e
+
+    def y_block(e):
+        return other - 2 * (e - 1)
+
+    def y_valid(e):
+        return (e - 1 >= 1 - side) & (e - 1 <= deep)
+
+    def forward(e):
+        @pl.when(e <= deep)
         def _():
-            onward(block).start()
-
-        @pl.when(mine == 1)
+            block = z_block(e)
+            arrived(piece(block, core), d_recv.at[block, core])
+
+            @pl.when(deep < last_deep)
+            def _():
+                onward(block).start()
+
+            across(block).start()
+            near(block).start()
+
+        @pl.when(y_valid(e))
         def _():
-            across(block).start()
-
-        near(block).start()
-
-    def ready(j):
-        block, _ = block_of(j)
+            block = y_block(e)
+            arrived(piece(block, core), d_recv.at[block, core])
+            near(block).start()
+
+    def ready(block):
         arrived(piece(block, 1 - core), d_recv.at[block, 1 - core])
         prepare(block)
-
-    def one_block(j, _):
-        forward(j)
-
-        @pl.when(j > 1)
-        def _():
-            ready(j - 1)
-            all_rows(False)
-
-        return 0
 
     @pl.when(shard > 0)
     def _():
@@ -515,21 +556,52 @@
 
     lax.fori_loop(0, rows // LANES, pool, 0)
 
-    lax.fori_loop(1, shard + 1, one_block, 0)
-
-    arrived(piece(shard, 1 - core), d_recv.at[shard, 1 - core])
-    prepare(shard)
-    all_rows(True)
-
-    @pl.when(shard > 0)
+    forward(1)
+
+    for step in range(1, chips):
+        g = place(behind(step), core)
+        arrived(qx.at[g], q_recv.at[g])
+        copy = remote(qx.at[g], qx.at[g], q_relay_send.at[step - 1], q_recv.at[g], {"tp": partner})
+        copy.start()
+        sends.append(copy)
+    for k in range(chips):
+        g = place(k, 1 - core)
+        arrived(qx.at[g], q_recv.at[g])
+
+    lax.fori_loop(0, 2, make_queries, 0)
+
+    ready(shard)
+    early_rows(shard, True)
+
+    def reach(e):
+        return jnp.minimum(2 * deep, jnp.where(e == 1, 0, jnp.where(e == 2, 3, 2 * e)))
+
+    def one_event(e, _):
+        forward(e)
+
+        def one(i, _):
+            k = lax.div(i + 1, 2)
+            first = lax.rem(i, 2) == 1
+            block = jnp.where(first, z_block(k), y_block(k))
+
+            @pl.when(first | y_valid(k))
+            def _():
+                ready(block)
+                early_rows(block, False)
+
+            return 0
+
+        lax.fori_loop(reach(e - 1) + 1, reach(e) + 1, one, 0)
+        return 0
+
+    lax.fori_loop(2, deep + 2, one_event, 0)
+    final = y_block(deep + 1)
+    has_final = y_valid(deep + 1)
+
+    @pl.when(has_final)
     def _():
-        ready(shard)
-
-        def one(step, _):
-            accumulate(lax.rem(chip + step, chips), False)
-            return 0
-
-        lax.fori_loop(1, chips, one, 0)
+        ready(final)
+        far_rows(final, False)
 
     def finish(k):
         at = pl.ds(pl.multiple_of(k * q_tile, q_tile), q_tile)
@@ -569,9 +641,19 @@
             copy.start()
             sends.append(copy)
 
-    @pl.when(shard > 0)
-    def _():
-        accumulate(chip, False)
+    if keep:
+        accumulate(shard, chip, True)
+
+        def own_rows(block, _):
+            accumulate(block, chip, False)
+            return 0
+
+        lax.fori_loop(0, shard, own_rows, 0)
+    else:
+
+        @pl.when(has_final)
+        def _():
+            accumulate(final, chip, False)
 
     finish(chip)
     arrived(act_p.at[chip], act_recv.at[chip])
@@ -605,6 +687,15 @@
         return 0
 
     lax.fori_loop(0, shard + 1, drain, 0)
+
+
+def vmem_bytes(arrays):
+    total = 0
+    for shape, kind in arrays:
+        size = 2 if kind == bf16 else 4
+        minor = up_to(shape[-1], LANES) * up_to(shape[-2], 32 // size) * size
+        total += math.prod(shape[:-2]) * minor
+    return total
 
 
 def tables(n_sp, n_tp, rows):
@@ -646,17 +737,27 @@
     rows, chips = r * n_tp, n_tp // 2
     half = r * chips
     others = max(1, chips - 1)
-    qc, kc, pc = w_qlat.shape[1], w_kvlat.shape[1], w_pool_in.shape[1]
+    w_qlat, w_krope = w_qlat.T, w_krope.T
+    qc, kc, pc = w_qlat.shape[0], w_kvlat.shape[1], w_pool_in.shape[1]
     heads = w_kup.shape[1] // NOPE
     kvlat = w_kup.shape[0]
     hc = heads * VDIM
     qp = up_to(qc, LANES)
     vm = pl.BlockSpec(memory_space=pltpu.VMEM)
-    hbm = pl.BlockSpec(memory_space=pl.ANY)
-    scratch = [
+    hbm = pl.BlockSpec(memory_space=pltpu.MemorySpace.HBM)
+    small = [
+        in_gain.reshape(1, -1),
+        pool_gain.reshape(1, -1),
+        qlat_gain.reshape(-1, LANES),
+        kvlat_gain.reshape(1, -1),
+        qhead_gain.reshape(1, -1),
+        khead_gain.reshape(1, -1),
+    ] + [jnp.asarray(t) for t in tables(n_sp, n_tp, rows)]
+    def scratch_of(slots):
+      return [(t.shape, f32) for t in small] + [
         ((r, width), bf16),
         ((width, pc), bf16),
-        ((width, qc), bf16),
+        ((qc, width), bf16),
         ((width, kc), bf16),
         (w_krope.shape, bf16),
         (w_qup.shape, bf16),
@@ -669,6 +770,8 @@
         ((n_tp, heads * HEAD, qp), bf16),
         ((heads * NOPE, kvlat), bf16),
         ((kvlat, heads * LANES), bf16),
+        ((HEAD, LANES), f32),
+        ((HEAD, LANES), f32),
         ((n_tp, r, width), bf16),
         ((n_tp, rows, qp), bf16),
         ((2, chips, r, kc), bf16),
@@ -677,17 +780,19 @@
         ((n_sp, 2, half + ROPE, kvlat), bf16),
         ((rows + RIM, pc), bf16),
         ((heads, rows, LANES), bf16),
-        ((heads, LANES, rows), bf16),
-        ((heads, rows, LANES), bf16),
+        ((slots, heads, LANES, rows), bf16),
+        ((slots, heads, rows, LANES), bf16),
         ((heads, rows, LANES), f32),
         ((rows, pc + hc), bf16),
         ((chips, r, pc + hc), bf16),
         ((others, COLS, r, width // COLS), bf16),
         ((others, COLS, r, width // COLS), bf16),
     ]
+    keep = vmem_bytes(scratch_of(n_sp)) + SPARE <= VMEM_MOST
+    scratch = scratch_of(n_sp if keep else 1)
     dma = pltpu.SemaphoreType.DMA
     sems = [
-        (10,),
+        (22,),
         (others, CHUNKS),
         (CHUNKS,),
         (others, CHUNKS),
@@ -711,24 +816,16 @@
         (others, COLS),
         (others, COLS),
     ]
-    small = [
-        in_gain.reshape(1, -1),
-        pool_gain.reshape(1, -1),
-        qlat_gain.reshape(-1, 1),
-        kvlat_gain.reshape(1, -1),
-        qhead_gain.reshape(-1, 1),
-        khead_gain.reshape(-1, 1),
-    ] + [jnp.asarray(t) for t in tables(n_sp, n_tp, rows)]
     return pl.pallas_call(
-        functools.partial(mixer_kernel, n_sp, n_tp),
+        functools.partial(mixer_kernel, n_sp, n_tp, keep),
         out_shape=jax.ShapeDtypeStruct((r, width), bf16),
-        in_specs=[hbm] * 10 + [vm] * len(small),
+        in_specs=[hbm] * (10 + len(small)),
         out_specs=vm,
         scratch_shapes=[pltpu.VMEM(s, d) for s, d in scratch] + [dma if s is None else dma(s) for s in sems],
         compiler_params=pltpu.CompilerParams(
-            collective_id=0, has_side_effects=True, vmem_limit_bytes=67_043_328
+            collective_id=0, has_side_effects=True, vmem_limit_bytes=min(VMEM_MOST, vmem_bytes(scratch) + SPARE)
         ),
-    )(
+    )(*[pltpu.with_memory_space_constraint(t, pltpu.MemorySpace.HBM) for t in (
         activations,
         w_pool_in,
         w_qlat,
@@ -739,7 +836,7 @@
         w_vup,
         w_out_pool,
         w_out_attn,
-        *small,
+        *small)]
     )
 
 

time: 131 us -> 97 us (0.74)
  Pallas kernels: 119 us -> 95 us
  local copies, waits for them, and re-layouts: 9.71 us -> 0.88 us
    pallas_call x1, Pallas kernels: 119 us -> 95 us  [local(): pl.pallas_call(functools.partial(mixer_kernel, n_sp, n_tp, keep), out_sha...]
    unnamed x5 -> x1, local copies, waits for them, and re-layouts: 5.3 us -> 0.88 us
    reshape x3 -> x0, local copies, waits for them, and re-layouts: 4.41 us -> none  [the longest x1 1.6 us: local(): qlat_gain.reshape(-1, 1)]
where the time goes in v2:
time: 97 us; the launch traced here: 95.8 us
  Pallas kernels  95 us (98%)
    pallas_call x1, Pallas kernels, local(): pl.pallas_call(functools.partial(mixer_kernel, n_sp, n_tp, keep), out_sha...  95 us

profile of v2, /device:TPU:28, one launch (start us, length us, event | category | flops | bytes accessed | tf_op | source)
XLA Modules:
  0.0 95.8 jit_solution(5534722790103792214)
XLA Ops:
  0.0 95.0 %shard_map.208 = bf16[192,2048]{1,0:T(8,128)(2,1)S(1)} custom-call(bf16[192,2048]{1,0:T(8,128)(2,1)} %x_hbm.1, bf16[2048,256]{1,0:T(8,128)(2,1)} %wpool_hbm.1, bf16[192,2048]{1,0:T(8,128)(2,1)} %bitcast.8, bf16[2048,128]{1,0:T(8,128)(2,1)} %wkv_hbm.1, bf16[32,2048]{1,0:T(8,128)(2,1)} %bitcast.9, bf16[768,384]{1,0:T(8,128)(2,1)} %wqup_hbm.1, ...), custom_call_target="tpu_custom_call" | custom-call | tf_op jit(solution)/shard_map/pallas_call | solution.py:819
  95.0 0.9 copy.24

commit v3 on v2

--- a/solution.py
+++ b/solution.py
@@ -152,6 +152,7 @@
     up_send,
     side_send,
     near_send,
+    x_send,
     d_recv,
     p_send,
     p_recv,
@@ -276,23 +277,48 @@
     wq_cat[...] = padded_transpose(wq_raw[...]).astype(bf16)
     loads["wpool"].wait()
 
-    def project(k, c, off, count, same_core):
-        g = place(k, c)
-        xs = xg[g, pl.ds(off, count), :]
-        at = rows_at(g, off, count)
-        both = dot(xs, wkv_cat[...])
+    def project_kv(k, c, off, count, same_core):
+        both = dot(xg[place(k, c), pl.ds(off, count), :], wkv_cat[...])
         kv_mine[c, k, pl.ds(off, count), :] = both[:, :kc].astype(bf16)
         if same_core:
             shared = both[:, LANES : 2 * LANES].astype(bf16).astype(f32)
             rope_own[pl.ds(pl.multiple_of(k * r + off, 8), count), :] = shared
-        qx[me, at, :] = dot(xs, wq_cat[...]).astype(bf16)
+
+    def project_q(k, c, off, count):
+        g = place(k, c)
+        qx[me, rows_at(g, off, count), :] = dot(xg[g, pl.ds(off, count), :], wq_cat[...]).astype(bf16)
+
+    def project_pool(k, c, off, count):
+        g = place(k, c)
         at_ext = pl.ds(pl.multiple_of(g * r + off + RIM, 16), count)
-        pool_ext[at_ext, :] = dot(xs, wpool[...]).astype(bf16)
+        pool_ext[at_ext, :] = dot(xg[g, pl.ds(off, count), :], wpool[...]).astype(bf16)
+
+    def project(k, c, off, count, same_core):
+        project_kv(k, c, off, count, same_core)
+        project_q(k, c, off, count)
+        project_pool(k, c, off, count)
+
+    def kv_piece(source, k, off, count):
+        return kvx.at[source, k, pl.ds(off, count), :]
+
+    def send_kv(k, off, count, number):
+        for step in range(1, n_tp):
+            there = lax.rem(me + step, n_tp)
+            copy = remote(
+                kv_mine.at[lax.rem(there, 2), k, pl.ds(off, count), :],
+                kv_piece(me, k, off, count),
+                kv_send.at[step - 1, number],
+                kv_recv.at[me, number],
+                {"tp": there},
+            )
+            copy.start()
+            sends.append(copy)
 
     project(chip, core, 0, r, True)
     for c in range(CHUNKS):
         arrived(xg.at[partner, pl.ds(c * rc, rc), :], a_recv.at[partner, c])
     project(chip, 1 - core, 0, r, False)
+    send_kv(chip, 0, r, 0)
 
     loads["wqup"].wait()
     for name in small:
@@ -330,19 +356,24 @@
             copy.start()
             sends.append(copy)
         for step in range(1, chips):
-            project(behind(step), core, c * rc, rc, True)
+            project_kv(behind(step), core, c * rc, rc, True)
+        if c < CHUNKS - 1:
+            for step in range(1, chips):
+                project_q(behind(step), core, c * rc, rc)
+                project_pool(behind(step), core, c * rc, rc)
         for step in range(1, chips):
             g = place(behind(step), 1 - core)
             arrived(xg.at[g, at, :], a_recv.at[g, c])
-            project(behind(step), 1 - core, c * rc, rc, False)
-
-    for step in range(1, n_tp):
-        there = lax.rem(me + step, n_tp)
-        copy = remote(
-            kv_mine.at[lax.rem(there, 2)], kvx.at[me], kv_send.at[step - 1], kv_recv.at[me], {"tp": there}
-        )
-        copy.start()
-        sends.append(copy)
+            project_kv(behind(step), 1 - core, c * rc, rc, False)
+            send_kv(behind(step), c * rc, rc, 1 + (step - 1) * CHUNKS + c)
+            if c < CHUNKS - 1:
+                project_q(behind(step), 1 - core, c * rc, rc)
+                project_pool(behind(step), 1 - core, c * rc, rc)
+    late = (CHUNKS - 1) * rc
+    for step in range(1, chips):
+        project_q(behind(step), core, late, rc)
+        project_q(behind(step), 1 - core, late, rc)
+
     own_q = qx.at[me]
     for step in range(1, chips):
         copy = remote(own_q, own_q, q_far_send.at[step - 1], q_recv.at[me], {"tp": place(ahead(step), core)})
@@ -352,6 +383,10 @@
     copy.start()
     sends.append(copy)
 
+    for step in range(1, chips):
+        project_pool(behind(step), core, late, rc)
+        project_pool(behind(step), 1 - core, late, rc)
+
     rim_copy = remote(
         pool_ext.at[pl.ds(rows, RIM), :], pool_ext.at[pl.ds(0, RIM), :], p_send, p_recv, {"sp": shard + 1}
     )
@@ -367,39 +402,75 @@
     kvx[me] = kv_mine[core]
     for step in range(1, n_tp):
         source = lax.rem(me + step, n_tp)
-        arrived(kvx.at[source], kv_recv.at[source])
-    lat = jnp.concatenate([kvx[i].reshape(half, kc).astype(f32) for i in range(n_tp)], axis=1)
+        its_chip = lax.div(source, 2)
+        arrived(kv_piece(source, its_chip, 0, r), kv_recv.at[source, 0])
+        for hop in range(1, chips):
+            k = lax.rem(its_chip + chips - hop, chips)
+            for c in range(CHUNKS):
+                number = 1 + (hop - 1) * CHUNKS + c
+                arrived(kv_piece(source, k, c * rc, rc), kv_recv.at[source, number])
+    p = crossed(r)
+
+    def permuted(x):
+        width = x.shape[2]
+        return jnp.concatenate(
+            [x[:, :p].reshape(chips * p, width), x[:, p:].reshape(chips * (r - p), width)], axis=0
+        )
+
+    lat = jnp.concatenate([permuted(kvx[i].astype(f32)) for i in range(n_tp)], axis=1)
     factor = lax.rsqrt(jnp.mean(lat * lat, axis=1, keepdims=True) + norm_eps)
     kv_all[shard, core, pl.ds(0, half), :] = (lat * factor * kvlat_gain[...]).astype(bf16)
-    kv_all[shard, core, pl.ds(half, ROPE), pl.ds(0, half)] = rope_own[...].T[:ROPE].astype(bf16)
-
-    def piece(block, h):
-        return kv_all.at[block, h]
-
-    def onward(block):
+    kv_all[shard, core, pl.ds(half, ROPE), pl.ds(0, half)] = permuted(rope_own[...].reshape(chips, r, LANES)).T[:ROPE].astype(bf16)
+
+    tail = chips * p
+
+    def head_rows(block, h, k):
+        return kv_all.at[block, h, pl.ds(pl.multiple_of(k * p, 16), p), :]
+
+    def tail_rows(block, h):
+        return kv_all.at[block, h, pl.ds(tail, half - tail + ROPE), :]
+
+    def parts_of(block):
+        return (head_rows(block, core, chip), tail_rows(block, core))
+
+    def to_shard(block, i, send, there):
+        ref = parts_of(block)[i]
+        sem = d_recv.at[block, core, chip if i == 0 else chips]
+        return remote(ref, ref, send.at[block, i], sem, {"sp": there})
+
+    def onward(block, i):
+        return to_shard(block, i, up_send, shard + 2)
+
+    def across(block, i):
+        return to_shard(block, i, side_send, other)
+
+    def over(block, step):
+        ref = head_rows(block, core, chip)
         return remote(
-            piece(block, core), piece(block, core), up_send.at[block], d_recv.at[block, core], {"sp": shard + 2}
+            ref, ref, x_send.at[block, step - 1], d_recv.at[block, core, chip], {"tp": place(ahead(step), core)}
         )
 
-    def across(block):
-        return remote(
-            piece(block, core), piece(block, core), side_send.at[block], d_recv.at[block, core], {"sp": other}
-        )
-
-    def near(block):
-        return remote(
-            piece(block, core), piece(block, core), near_send.at[block], d_recv.at[block, core], {"tp": partner}
-        )
-
-    @pl.when(deep < last_deep)
-    def _():
-        onward(shard).start()
-
-    @pl.when(side == 0)
-    def _():
-        across(shard).start()
-
-    near(shard).start()
+    def near(block, k):
+        ref = head_rows(block, core, k)
+        return remote(ref, ref, near_send.at[block, k], d_recv.at[block, core, k], {"tp": partner})
+
+    def near_tail(block):
+        ref = tail_rows(block, core)
+        return remote(ref, ref, near_send.at[block, chips], d_recv.at[block, core, chips], {"tp": partner})
+
+    for i in range(2):
+
+        @pl.when(deep < last_deep)
+        def _():
+            onward(shard, i).start()
+
+        @pl.when(side == 0)
+        def _():
+            across(shard, i).start()
+
+    for k in range(chips):
+        near(shard, k).start()
+    near_tail(shard).start()
 
     score_scale = HEAD ** (-0.5) * math.log2(math.e)
     q_tile = 2 * r
@@ -466,11 +537,15 @@
                 v = jnp.where(lane == VDIM, 1.0, value[:, h * LANES : (h + 1) * LANES])
                 values[slot, h, at, :] = v.astype(bf16)
 
-    key_tile = math.gcd(half, 384)
+    key_tile = math.gcd(rows, 256)
+    runs = key_runs(n_tp, r)
 
     def accumulate(block, i, masked):
+        attend(block, i * q_tile, q_tile, masked)
+
+    def attend(block, row, count, masked):
         slot = block if keep else 0
-        at = pl.ds(pl.multiple_of(i * q_tile, q_tile), q_tile)
+        at = pl.ds(pl.multiple_of(row, r), count)
         for h in range(heads):
             q = queries[h, at, :]
             total = acc[h, at, :]
@@ -478,11 +553,14 @@
                 cols = pl.ds(j * key_tile, key_tile)
                 weights = jnp.exp2(dot(q, keys_t[slot, h, :, cols]))
                 if masked:
-                    q_pos = i * q_tile + lax.broadcasted_iota(jnp.int32, weights.shape, 0)
-                    col = (j * key_tile) % half + lax.broadcasted_iota(jnp.int32, weights.shape, 1)
-                    k_pos = col + ((j * key_tile) // half) * r
-                    for k in range(1, chips):
-                        k_pos = k_pos + jnp.where(col >= k * r, r, 0)
+                    q_pos = row + lax.broadcasted_iota(jnp.int32, weights.shape, 0)
+                    col = j * key_tile + lax.broadcasted_iota(jnp.int32, weights.shape, 1)
+                    k_pos = col
+                    shift = 0
+                    for start, first in runs:
+                        if first - start != shift and start < (j + 1) * key_tile:
+                            k_pos = k_pos + jnp.where(col >= start, first - start - shift, 0)
+                            shift = first - start
                     weights = jnp.where(k_pos <= q_pos, weights, 0.0)
                 total = total + dot(weights.astype(bf16), values[slot, h, cols, :])
             acc[h, at, :] = total
@@ -508,27 +586,42 @@
     def y_valid(e):
         return (e - 1 >= 1 - side) & (e - 1 <= deep)
 
+    def pass_on(block, from_z):
+        for i in range(2):
+            arrived(parts_of(block)[i], d_recv.at[block, core, chip if i == 0 else chips])
+            if from_z:
+
+                @pl.when(deep < last_deep)
+                def _():
+                    onward(block, i).start()
+
+                across(block, i).start()
+            if i == 0:
+                for step in range(1, chips):
+                    over(block, step).start()
+                near(block, chip).start()
+            else:
+                near_tail(block).start()
+
     def forward(e):
         @pl.when(e <= deep)
         def _():
-            block = z_block(e)
-            arrived(piece(block, core), d_recv.at[block, core])
-
-            @pl.when(deep < last_deep)
-            def _():
-                onward(block).start()
-
-            across(block).start()
-            near(block).start()
+            pass_on(z_block(e), True)
 
         @pl.when(y_valid(e))
         def _():
-            block = y_block(e)
-            arrived(piece(block, core), d_recv.at[block, core])
-            near(block).start()
+            pass_on(y_block(e), False)
+
+    def relay(block):
+        for step in range(1, chips):
+            k = behind(step)
+            arrived(head_rows(block, core, k), d_recv.at[block, core, k])
+            near(block, k).start()
 
     def ready(block):
-        arrived(piece(block, 1 - core), d_recv.at[block, 1 - core])
+        for k in range(chips):
+            arrived(head_rows(block, 1 - core, k), d_recv.at[block, 1 - core, k])
+        arrived(tail_rows(block, 1 - core), d_recv.at[block, 1 - core, chips])
         prepare(block)
 
     @pl.when(shard > 0)
@@ -574,23 +667,35 @@
     early_rows(shard, True)
 
     def reach(e):
-        return jnp.minimum(2 * deep, jnp.where(e == 1, 0, jnp.where(e == 2, 3, 2 * e)))
+        return 2 * (e - 1)
 
     def one_event(e, _):
         forward(e)
 
-        def one(i, _):
+        def pick(i):
             k = lax.div(i + 1, 2)
             first = lax.rem(i, 2) == 1
-            block = jnp.where(first, z_block(k), y_block(k))
-
-            @pl.when(first | y_valid(k))
+            return jnp.where(first, z_block(k), y_block(k)), first | y_valid(k)
+
+        def relay_at(i):
+            block, valid = pick(i)
+
+            @pl.when(valid & (i <= reach(e)))
+            def _():
+                relay(block)
+
+        def one(i, _):
+            relay_at(i + 1)
+            block, valid = pick(i)
+
+            @pl.when(valid)
             def _():
                 ready(block)
                 early_rows(block, False)
 
             return 0
 
+        relay_at(reach(e - 1) + 1)
         lax.fori_loop(reach(e - 1) + 1, reach(e) + 1, one, 0)
         return 0
 
@@ -600,22 +705,30 @@
 
     @pl.when(has_final)
     def _():
+        relay(final)
         ready(final)
-        far_rows(final, False)
-
-    def finish(k):
-        at = pl.ds(pl.multiple_of(k * q_tile, q_tile), q_tile)
+
+    def finish(k, c):
+        at = rows_at(place(k, c), 0, r)
         parts = []
         for h in range(heads):
             a = acc[h, at, :]
             parts.append(a[:, :VDIM] / a[:, VDIM : VDIM + 1])
         act[at, pc:] = jnp.concatenate(parts, axis=1).astype(bf16)
+
+    def hand_over(k):
+        finish(k, 1 - core)
         copy = remote(
             act.at[rows_at(place(k, 1 - core), 0, r), :], act_p.at[k], act_send.at[k], act_recv.at[k], {"tp": partner}
         )
         copy.start()
         sends.append(copy)
 
+    def last_block(k, c):
+        @pl.when(has_final)
+        def _():
+            attend(final, place(k, c) * r, r, False)
+
     cw = width // COLS
 
     def product(k, n):
@@ -624,7 +737,11 @@
         return dot(mine, wo[:, cols]) + dot(act_p[k], wo_p[:, cols])
 
     for step in range(1, chips):
-        finish(ahead(step))
+        last_block(ahead(step), 1 - core)
+        hand_over(ahead(step))
+    for step in range(1, chips):
+        last_block(ahead(step), core)
+        finish(ahead(step), core)
     arrived(wo_p, wo_recv)
     for step in range(1, chips):
         k = ahead(step)
@@ -655,7 +772,8 @@
         def _():
             accumulate(final, chip, False)
 
-    finish(chip)
+    hand_over(chip)
+    finish(chip, core)
     arrived(act_p.at[chip], act_recv.at[chip])
     for n in range(COLS):
         total = product(chip, n)
@@ -674,15 +792,25 @@
 
     def drain(j, _):
         block = shard - j
-        near(block).wait_send()
-
-        @pl.when((lax.rem(j, 2) == 0) & (deep < last_deep))
+        column = lax.rem(j, 2) == 0
+        for k in range(chips):
+            near(block, k).wait_send()
+        near_tail(block).wait_send()
+
+        @pl.when(j > 0)
         def _():
-            onward(block).wait_send()
-
-        @pl.when((lax.rem(j, 2) == 0) & ((j > 0) | (side == 0)))
-        def _():
-            across(block).wait_send()
+            for step in range(1, chips):
+                over(block, step).wait_send()
+
+        for i in range(2):
+
+            @pl.when(column & (deep < last_deep))
+            def _():
+                onward(block, i).wait_send()
+
+            @pl.when(column & ((j > 0) | (side == 0)))
+            def _():
+                across(block, i).wait_send()
 
         return 0
 
@@ -698,6 +826,20 @@
     return total
 
 
+def crossed(r):
+    return r * 5 // 6
+
+
+def key_runs(n_tp, r):
+    chips, p = n_tp // 2, crossed(r)
+    runs = []
+    for c in range(2):
+        base = c * chips * r
+        runs += [(base + k * p, (2 * k + c) * r) for k in range(chips)]
+        runs += [(base + chips * p + k * (r - p), (2 * k + c) * r + p) for k in range(chips)]
+    return runs
+
+
 def tables(n_sp, n_tp, rows):
     frequency = np.float32(rope_theta) ** (-np.arange(0, ROPE, 2, dtype=np.float32) / np.float32(ROPE))
     r = rows // n_tp
@@ -708,7 +850,8 @@
         return np.cos(angles).astype(np.float32), np.sin(angles).astype(np.float32)
 
     natural = np.arange(rows)
-    split = natural.reshape(n_tp // 2, 2, r).transpose(1, 0, 2).reshape(-1)
+    runs = key_runs(n_tp, r) + [(rows, 0)]
+    split = np.concatenate([first + np.arange(runs[i + 1][0] - at) for i, (at, first) in enumerate(runs[:-1])])
     blocks = make(np.arange(n_sp) * rows)
     columns = [np.ascontiguousarray(t.T)[:, :, None] for t in blocks]
     return [*make(natural), *make(split), *columns]
@@ -797,16 +940,17 @@
         (CHUNKS,),
         (others, CHUNKS),
         (n_tp, CHUNKS),
-        (n_tp,),
-        (n_tp,),
+        (n_tp, 1 + others * CHUNKS),
+        (n_tp, 1 + others * CHUNKS),
         (others,),
         None,
         (others,),
         (n_tp,),
-        (n_sp,),
-        (n_sp,),
-        (n_sp,),
         (n_sp, 2),
+        (n_sp, 2),
+        (n_sp, chips + 1),
+        (n_sp, others),
+        (n_sp, 2, chips + 1),
         None,
         None,
         None,

time: 97 us -> 87 us (0.90); the launches traced: 95.8 us -> 86.9 us
  Pallas kernels: 95 us -> 86 us
    pallas_call x1, Pallas kernels: 95 us -> 86 us  [local(): pl.pallas_call(functools.partial(mixer_kernel, n_sp, n_tp, keep), out_sha...]
where the time goes in v3:
time: 87 us; the launch traced here: 86.9 us
  Pallas kernels  86 us (99%)
  local copies, waits for them, and re-layouts  0.88 us (1%)
    pallas_call x1, Pallas kernels, local(): pl.pallas_call(functools.partial(mixer_kernel, n_sp, n_tp, keep), out_sha...  86 us

profile of v3, /device:TPU:28, one launch (start us, length us, event | category | flops | bytes accessed | tf_op | source)
XLA Modules:
  0.0 86.9 jit_solution(10698253214486492924)
XLA Ops:
  0.0 86.0 %shard_map.208 = bf16[192,2048]{1,0:T(8,128)(2,1)S(1)} custom-call(bf16[192,2048]{1,0:T(8,128)(2,1)} %x_hbm.1, bf16[2048,256]{1,0:T(8,128)(2,1)} %wpool_hbm.1, bf16[192,2048]{1,0:T(8,128)(2,1)} %bitcast.8, bf16[2048,128]{1,0:T(8,128)(2,1)} %wkv_hbm.1, bf16[32,2048]{1,0:T(8,128)(2,1)} %bitcast.9, bf16[768,384]{1,0:T(8,128)(2,1)} %wqup_hbm.1, ...), custom_call_target="tpu_custom_call" | custom-call | tf_op jit(solution)/shard_map/pallas_call | solution.py:963
  86.0 0.9 %copy.24 = bf16[192,2048]{1,0:T(8,128)(2,1)} copy(bf16[192,2048]{1,0:T(8,128)(2,1)S(1)} %shard_map.208) | data formatting | bytes 1572864

commit v4 on v3

--- a/solution.py
+++ b/solution.py
@@ -125,6 +125,7 @@
     gain_k,
     xg,
     qx,
+    qy,
     kv_mine,
     kvx,
     rope_own,
@@ -183,6 +184,14 @@
     hc = heads * VDIM
     rc = r // CHUNKS
 
+    packed = packs(qc, chips)
+
+    def doubled(w):
+        if not packed:
+            return w
+        rest = w[:, LANES:]
+        return jnp.concatenate([w[:, :LANES], rest + pltpu.roll(rest, LANES // 2, 1)], axis=1)
+
     loads = {}
 
     def load(i, name, src, dst):
@@ -274,7 +283,7 @@
     wkv_cat[:, :kc] = wkv_raw[...]
     wkv_cat[:, LANES:] = padded_transpose(wkr_raw[...]).astype(bf16)
     loads["wq"].wait()
-    wq_cat[...] = padded_transpose(wq_raw[...]).astype(bf16)
+    wq_cat[...] = doubled(padded_transpose(wq_raw[...])).astype(bf16)
     loads["wpool"].wait()
 
     def project_kv(k, c, off, count, same_core):
@@ -286,7 +295,14 @@
 
     def project_q(k, c, off, count):
         g = place(k, c)
-        qx[me, rows_at(g, off, count), :] = dot(xg[g, pl.ds(off, count), :], wq_cat[...]).astype(bf16)
+        q = dot(xg[g, pl.ds(off, count), :], wq_cat[...]).astype(bf16)
+        if packed:
+            at = pl.ds(pl.multiple_of(k * r + off, 16), count)
+            side_of = lax.broadcasted_iota(jnp.int32, (count, LANES), 1) // (LANES // 2)
+            old, new = qy[me, at, :].astype(f32), q[:, LANES:].astype(f32)
+            qy[me, at, :] = jnp.where(side_of == c, new, old).astype(bf16)
+            q = q[:, :LANES]
+        qx[me, rows_at(g, off, count), :] = q
 
     def project_pool(k, c, off, count):
         g = place(k, c)
@@ -330,7 +346,7 @@
     for src in range(n_tp):
         span = slice(src * qc, (src + 1) * qc)
         part = wqup[span, :].astype(f32) * lat_gain[span, :1]
-        wq_t[src] = padded_transpose(part).astype(bf16)
+        wq_t[src] = doubled(padded_transpose(part)).astype(bf16)
     loads["wkup"].wait()
     wk_t[...] = padded_transpose(wkup[...]).astype(bf16)
     loads["wvup"].wait()
@@ -374,14 +390,20 @@
         project_q(behind(step), core, late, rc)
         project_q(behind(step), 1 - core, late, rc)
 
-    own_q = qx.at[me]
-    for step in range(1, chips):
-        copy = remote(own_q, own_q, q_far_send.at[step - 1], q_recv.at[me], {"tp": place(ahead(step), core)})
+    q_parts = (qx, qy) if packed else (qx,)
+    for i, whole in enumerate(q_parts):
+        own_q = whole.at[me]
+        for step in range(1, chips):
+            copy = remote(
+                own_q, own_q, q_far_send.at[step - 1, i], q_recv.at[me, i], {"tp": place(ahead(step), core)}
+            )
+            copy.start()
+            sends.append(copy)
+    for i, whole in enumerate(q_parts):
+        own_q = whole.at[me]
+        copy = remote(own_q, own_q, q_near_send.at[i], q_recv.at[me, i], {"tp": partner})
         copy.start()
         sends.append(copy)
-    copy = remote(own_q, own_q, q_near_send, q_recv.at[me], {"tp": partner})
-    copy.start()
-    sends.append(copy)
 
     for step in range(1, chips):
         project_pool(behind(step), core, late, rc)
@@ -484,9 +506,14 @@
         at = pl.ds(pl.multiple_of(i * half, half), half)
         raw = None
         squares = None
-        ones = jnp.ones((8, qx.shape[2]), bf16)
+        ones = jnp.ones((8, wq_t.shape[2]), bf16)
         for src in range(n_tp):
             part = qx[src, at, :]
+            if packed:
+                rest = qy[src, pl.ds(pl.multiple_of(i * r, r), r), :].astype(f32)
+                side_of = lax.broadcasted_iota(jnp.int32, rest.shape, 1) // (LANES // 2)
+                rest = [jnp.where(side_of == c, rest, 0.0).astype(bf16) for c in range(2)]
+                part = jnp.concatenate([part, jnp.concatenate(rest, axis=0)], axis=1)
             term = dot_nt(wq_t[src], part)
             raw = term if raw is None else raw + term
             pf = part.astype(f32)
@@ -651,15 +678,18 @@
 
     forward(1)
 
-    for step in range(1, chips):
-        g = place(behind(step), core)
-        arrived(qx.at[g], q_recv.at[g])
-        copy = remote(qx.at[g], qx.at[g], q_relay_send.at[step - 1], q_recv.at[g], {"tp": partner})
-        copy.start()
-        sends.append(copy)
-    for k in range(chips):
-        g = place(k, 1 - core)
-        arrived(qx.at[g], q_recv.at[g])
+    for i, whole in enumerate(q_parts):
+        for step in range(1, chips):
+            block = whole.at[place(behind(step), core)]
+            sem = q_recv.at[place(behind(step), core), i]
+            arrived(block, sem)
+            copy = remote(block, block, q_relay_send.at[step - 1, i], sem, {"tp": partner})
+            copy.start()
+            sends.append(copy)
+    for i, whole in enumerate(q_parts):
+        for k in range(chips):
+            g = place(k, 1 - core)
+            arrived(whole.at[g], q_recv.at[g, i])
 
     lax.fori_loop(0, 2, make_queries, 0)
 
@@ -824,6 +854,10 @@
         minor = up_to(shape[-1], LANES) * up_to(shape[-2], 32 // size) * size
         total += math.prod(shape[:-2]) * minor
     return total
+
+
+def packs(qc, chips):
+    return chips == 2 and qc == LANES + LANES // 2
 
 
 def crossed(r):
@@ -916,7 +950,8 @@
         ((HEAD, LANES), f32),
         ((HEAD, LANES), f32),
         ((n_tp, r, width), bf16),
-        ((n_tp, rows, qp), bf16),
+        ((n_tp, rows, LANES if packs(qc, chips) else qp), bf16),
+        ((n_tp, half, LANES), bf16),
         ((2, chips, r, kc), bf16),
         ((n_tp, chips, r, kc), bf16),
         ((half, LANES), f32),
@@ -942,10 +977,10 @@
         (n_tp, CHUNKS),
         (n_tp, 1 + others * CHUNKS),
         (n_tp, 1 + others * CHUNKS),
-        (others,),
-        None,
-        (others,),
-        (n_tp,),
+        (others, 2),
+        (2,),
+        (others, 2),
+        (n_tp, 2),
         (n_sp, 2),
         (n_sp, 2),
         (n_sp, chips + 1),

time: 87 us -> 86.6 us (level)
  no operation moved by 1% of the time
where the time goes in v4:
time: 86.6 us; the launch traced here: 86.4 us
  Pallas kernels  85.5 us (99%)
  local copies, waits for them, and re-layouts  0.88 us (1%)
    pallas_call x1, Pallas kernels, local(): pl.pallas_call(functools.partial(mixer_kernel, n_sp, n_tp, keep), out_sha...  85.5 us

profile of v4, /device:TPU:28, one launch (start us, length us, event | category | flops | bytes accessed | tf_op | source)
XLA Modules:
  0.0 86.4 jit_solution(10704275371551583620)
XLA Ops:
  0.0 85.5 %shard_map.208 = bf16[192,2048]{1,0:T(8,128)(2,1)S(1)} custom-call(bf16[192,2048]{1,0:T(8,128)(2,1)} %x_hbm.1, bf16[2048,256]{1,0:T(8,128)(2,1)} %wpool_hbm.1, bf16[192,2048]{1,0:T(8,128)(2,1)} %bitcast.8, bf16[2048,128]{1,0:T(8,128)(2,1)} %wkv_hbm.1, bf16[32,2048]{1,0:T(8,128)(2,1)} %bitcast.9, bf16[768,384]{1,0:T(8,128)(2,1)} %wqup_hbm.1, ...), custom_call_target="tpu_custom_call" | custom-call | tf_op jit(solution)/shard_map/pallas_call | solution.py:998
  85.5 0.9 %copy.24 = bf16[192,2048]{1,0:T(8,128)(2,1)} copy(bf16[192,2048]{1,0:T(8,128)(2,1)S(1)} %shard_map.208) | data formatting | bytes 1572864
